TPU v7x, 32 devices: a whole 2x2x4 slice. The times are simulated.
32 devices in a mesh: grp: 2 (over y), sp: 4 (over z), fs: 2 (over x), tp: 2 (over core).
Axes of the slice: x: 2, y: 2, z: 4, core: 2. Of those that a mesh axis runs over, the one named last changes fastest.
Arguments:
- tokens: bfloat16 [4, 512, 2048], P(('grp', 'fs'), 'sp', 'tp'), parts along dimension 0, may hold values from -120 to 120
- mix_gain: float32 [2048], replicated, may hold values from 0.1 to 1.9
- attn_query: bfloat16 [2048, 1024], P('fs', 'tp'), may hold values from -0.375 to 0.375
- attn_key: bfloat16 [2048, 1024], P('fs', 'tp'), may hold values from -0.125 to 0.125
- attn_value: bfloat16 [2048, 1024], P('fs', 'tp'), may hold values from -0.125 to 0.125
- rec_query: bfloat16 [2048, 1024], P('fs', 'tp'), may hold values from -0.125 to 0.125
- rec_forget: bfloat16 [2048, 1024], P('fs', 'tp'), may hold values from -0.125 to 0.125
- rec_input: bfloat16 [2048, 1024], P('fs', 'tp'), may hold values from -0.125 to 0.125
- break_offset: float32 [8], P('tp'), may hold values from -13.5 to -7
- forget_room: float32 [8, 128], P('tp'), may hold values from 0.0009765625 to 0.05
- out_gain: float32 [128], replicated, may hold values from 0.1 to 1.9
- out_attn: bfloat16 [1024, 2048], P('tp', 'fs'), may hold values from -0.125 to 0.125
- out_rec: bfloat16 [1024, 2048], P('tp', 'fs'), may hold values from -0.125 to 0.125
Outputs:
- mixed: bfloat16 [4, 512, 2048], P(('grp', 'fs'), ('sp', 'tp')), parts along dimension 0
There are 2 independent parts, one for each index of `grp`. A program takes and returns all parts, laid end to end along the dimension named above; an argument that names none is the same for every part. Nothing has to cross between parts.
All inputs are finite; a program needn't handle non-finite values.
Results may differ from a plain program's by a relative error of at most 0.019.
Values may be sent and summed in bfloat16 or wider, within the bound.
A program may use at most 64 MiB of HBM per device.

v0:
```python
import functools
import math

import jax
import jax.numpy as jnp
from jax import lax
from jax.experimental import pallas as pl
from jax.experimental.pallas import tpu as pltpu
from jax.sharding import PartitionSpec as P

LANES = 128
norm_eps = 1e-06
MESH = pl.DeviceIdType.MESH
F32 = jnp.float32
BF16 = jnp.bfloat16
N_PROJ = 6
GROUPS = 2
CHUNKS = 2


def dot_nn(a, b):
    return lax.dot_general(a, b, (((1,), (0,)), ((), ())), preferred_element_type=F32)


def dot_nt(a, b):
    return lax.dot_general(a, b, (((1,), (1,)), ((), ())), preferred_element_type=F32)


def dot_tn(a, b):
    return lax.dot_general(a, b, (((0,), (0,)), ((), ())), preferred_element_type=F32)


def halves(x):
    high = x.astype(BF16)
    return high, (x - high.astype(F32)).astype(BF16)


def kernel(
    n_sp, n_fs, n_tp,
    tok_hbm, gain, w_k, w_v, w_f, w_i, w_q, w_r, offs, room, out_gain, o_attn, o_rec,
    out,
    tok, wbuf, obuf, xt, xg, ss, acc, psend, precv, kv, qbuf, qdec, ecum, kinv,
    att, run, loc, st_loc, dec, st_in, st_out, heads, hrecv, part_acc, part, precv2, mix, mrecv,
    t_sem, w_sem, x_send, x_recv, f_send, ss_send, ss_recv, p_send, p_recv, kv_send, kv_recv,
    st_sem, h_send, h_recv, pp_send, pp_recv, m_send, m_recv,
):
    sp, fs, tp = lax.axis_index("sp"), lax.axis_index("fs"), lax.axis_index("tp")
    rows, feat_t = tok.shape
    feat_f = xt.shape[2]
    width = feat_t * n_tp
    cols = wbuf.shape[2]
    n_heads = cols // LANES
    share = rows // n_tp
    out_cols = obuf.shape[2]
    has_next = sp < n_sp - 1
    has_prev = sp > 0

    def fs_at(step):
        return lax.rem(fs + step, n_fs)

    def tp_at(step):
        return lax.rem(tp + step, n_tp)

    tok_copy = pltpu.make_async_copy(tok_hbm, tok, t_sem.at[0])
    tok_copy.start()
    w_copies = [
        pltpu.make_async_copy(w, wbuf.at[i], w_sem.at[i])
        for i, w in enumerate((w_k, w_v, w_f, w_i, w_q, w_r))
    ]
    w_copies += [
        pltpu.make_async_copy(w, obuf.at[i], w_sem.at[N_PROJ + i])
        for i, w in enumerate((o_attn, o_rec))
    ]
    barrier = pltpu.get_barrier_semaphore()
    for df in range(n_fs):
        for dt in range(n_tp):
            if df or dt:
                pl.semaphore_signal(
                    barrier, inc=1, device_id={"fs": fs_at(df), "tp": tp_at(dt)}, device_id_type=MESH
                )

    @pl.when(has_next)
    def _():
        pl.semaphore_signal(barrier, inc=1, device_id={"sp": sp + 1}, device_id_type=MESH)

    @pl.when(has_prev)
    def _():
        pl.semaphore_signal(barrier, inc=1, device_id={"sp": sp - 1}, device_id_type=MESH)

    for copy in w_copies:
        copy.start()
    tok_copy.wait()

    next_count = jnp.where(has_next, 1, 0)
    prev_count = jnp.where(has_prev, 1, 0)
    pl.semaphore_wait(barrier, n_fs * n_tp - 1 + next_count + prev_count)

    def holder(f_index):
        return (f_index * feat_f) // feat_t

    def x_copy(df, dt):
        dest = fs_at(df)
        start = pl.multiple_of(lax.rem(dest * feat_f, feat_t), LANES)
        part_rows = rows if df == 0 else share
        first = 0 if df == 0 else pl.multiple_of(tp_at(dt) * share, share)
        piece = tp if df == 0 else tp_at(dt)
        return pltpu.make_async_remote_copy(
            src_ref=tok.at[pl.ds(first, part_rows), pl.ds(start, feat_f)],
            dst_ref=xt.at[fs, pl.ds(first, part_rows)],
            send_sem=x_send.at[df * n_tp + dt],
            recv_sem=x_recv.at[fs * n_tp + piece],
            device_id={"fs": dest, "tp": tp_at(dt)},
            device_id_type=MESH,
        )

    def f_copy(df, dt):
        slot = fs_at(df)
        first = pl.multiple_of(tp * share, share)
        return pltpu.make_async_remote_copy(
            src_ref=xt.at[slot, pl.ds(first, share)],
            dst_ref=xt.at[slot, pl.ds(first, share)],
            send_sem=f_send.at[df * n_tp + dt],
            recv_sem=x_recv.at[slot * n_tp + tp],
            device_id={"tp": tp_at(dt)},
            device_id_type=MESH,
        )

    x_order = [(df, dt) for df in list(range(1, n_fs)) + [0] for dt in range(n_tp) if df or dt]
    for df, dt in x_order:
        @pl.when(holder(fs_at(df)) == tp)
        def _(df=df, dt=dt):
            x_copy(df, dt).start()

    squares = jnp.zeros((rows, LANES), F32)
    for c in range(feat_t // LANES):
        piece = tok[:, c * LANES:(c + 1) * LANES].astype(F32)
        squares = squares + piece * piece
    ss[tp] = squares

    def ss_copy(dt):
        return pltpu.make_async_remote_copy(
            src_ref=ss.at[tp], dst_ref=ss.at[tp],
            send_sem=ss_send.at[dt - 1], recv_sem=ss_recv.at[tp],
            device_id={"tp": tp_at(dt)}, device_id_type=MESH,
        )

    for dt in range(1, n_tp):
        ss_copy(dt).start()

    own_holder = holder(fs) == tp
    gain_f = gain[:, pl.ds(pl.multiple_of(fs * feat_f, LANES), feat_f)]

    @pl.when(own_holder)
    def _():
        start = pl.multiple_of(lax.rem(fs * feat_f, feat_t), LANES)
        xg[0] = (tok[:, pl.ds(start, feat_f)].astype(F32) * gain_f).astype(BF16)

    def x_wait(slot, piece, first, count):
        view = xt.at[slot, pl.ds(first, count)]
        pltpu.make_async_remote_copy(
            src_ref=view, dst_ref=view,
            send_sem=x_send.at[0], recv_sem=x_recv.at[slot * n_tp + piece],
            device_id={"tp": tp_at(1)}, device_id_type=MESH,
        ).wait_recv()

    g_cols = cols // GROUPS
    units = [(w, g * g_cols, g_cols) for g in range(GROUPS) for w in (0, 1)]
    units += [(w, 0, cols) for w in range(2, N_PROJ)]
    n_units = len(units)
    n_kv = 2 * GROUPS

    def p_copy(df, u):
        w, first, count = units[u]
        return pltpu.make_async_remote_copy(
            src_ref=psend.at[df - 1, w, :, pl.ds(first, count)],
            dst_ref=precv.at[df - 1, w, :, pl.ds(first, count)],
            send_sem=p_send.at[(df - 1) * n_units + u], recv_sem=p_recv.at[(df - 1) * n_units + u],
            device_id={"fs": fs_at(df)}, device_id_type=MESH,
        )

    def row_part(dt):
        return pl.ds(pl.multiple_of(tp_at(dt) * share, share), share)

    def first_copy(df, dt):
        index = (n_fs - 1) * n_units + (df - 1) * n_tp + dt
        return pltpu.make_async_remote_copy(
            src_ref=psend.at[df - 1, 0, row_part(dt), pl.ds(0, g_cols)],
            dst_ref=precv.at[df - 1, 0, row_part(dt), pl.ds(0, g_cols)],
            send_sem=p_send.at[index], recv_sem=p_recv.at[index],
            device_id={"fs": fs_at(df)}, device_id_type=MESH,
        )

    def first_part(df, dt):
        mine = row_part(dt)
        xg[df, mine, :] = (xt[fs_at(df), mine, :].astype(F32) * gain_f).astype(BF16)
        psend[df - 1, 0, mine, 0:g_cols] = dot_nn(xg[df, mine, :], wbuf[0, :, 0:g_cols]).astype(BF16)
        first_copy(df, dt).start()

    w_copies[0].wait()
    for df in range(1, n_fs):
        slot = fs_at(df)
        x_wait(slot, tp, pl.multiple_of(tp * share, share), share)
        for dt in range(1, n_tp):
            f_copy(df, dt).start()
        first_part(df, 0)
    for df in range(1, n_fs):
        slot = fs_at(df)
        for dt in range(1, n_tp):
            piece = tp_at(dt)
            x_wait(slot, piece, pl.multiple_of(piece * share, share), share)
            first_part(df, dt)
    for u, (w, first, count) in enumerate(units):
        if u == 0:
            continue
        if first == 0:
            w_copies[w].wait()
        cut = slice(first, first + count)
        for df in range(1, n_fs):
            psend[df - 1, w, :, cut] = dot_nn(xg[df], wbuf[w, :, cut]).astype(BF16)
            p_copy(df, u).start()

    @pl.when(jnp.logical_not(own_holder))
    def _():
        x_wait(fs, holder(fs), 0, rows)
        xg[0] = (xt[fs].astype(F32) * gain_f).astype(BF16)

    for w in range(N_PROJ):
        acc[w] = dot_nn(xg[0], wbuf[w])

    total = ss[tp]
    for dt in range(1, n_tp):
        other = tp_at(dt)
        pltpu.make_async_remote_copy(
            src_ref=ss.at[other], dst_ref=ss.at[other],
            send_sem=ss_send.at[dt - 1], recv_sem=ss_recv.at[other],
            device_id={"tp": other}, device_id_type=MESH,
        ).wait_recv()
        total = total + ss[other]
    factor = lax.rsqrt(jnp.sum(total, axis=1, keepdims=True) / width + norm_eps)

    def finish(u):
        w, first, count = units[u]
        cut = slice(first, first + count)
        value = acc[w, :, cut]
        for df in range(1, n_fs):
            if u == 0:
                for dt in range(n_tp):
                    first_copy(df, dt).wait_recv()
            else:
                p_copy(df, u).wait_recv()
            value = value + precv[df - 1, w, :, cut].astype(F32)
        return (value * factor).astype(BF16)

    def kv_copy(slot, c):
        return pltpu.make_async_remote_copy(
            src_ref=kv.at[slot, c], dst_ref=kv.at[slot, c],
            send_sem=kv_send.at[slot * n_kv + c], recv_sem=kv_recv.at[slot * n_kv + c],
            device_id={"sp": lax.rem(sp + 1, n_sp)}, device_id_type=MESH,
        )

    for c in range(n_kv):
        kv[sp, c] = finish(c)

        @pl.when(has_next)
        def _(c=c):
            kv_copy(sp, c).start()

    def hand_on(step, c):
        kv_copy(sp - step, c).wait_recv()

        @pl.when(has_next)
        def _():
            kv_copy(sp - step, c).start()

    def hand_on_if(step, c):
        if step < n_sp:
            pl.when(sp >= step)(functools.partial(hand_on, step, c))

    hand_on_if(1, 0)
    hand_on_if(1, 1)
    iota_r = lax.broadcasted_iota(jnp.int32, (rows, rows), 0)
    iota_c = lax.broadcasted_iota(jnp.int32, (rows, rows), 1)
    causal = iota_r >= iota_c
    strict = iota_c < iota_r

    def st_copy(h):
        return pltpu.make_async_remote_copy(
            src_ref=st_out.at[h], dst_ref=st_in.at[h],
            send_sem=st_sem.at[h], recv_sem=st_sem.at[n_heads + h],
            device_id={"sp": lax.rem(sp + 1, n_sp)}, device_id_type=MESH,
        )

    lower = jnp.where(causal, 1.0, 0.0).astype(BF16)
    forget_pre = finish(n_kv)
    for c in range(2, n_kv):
        hand_on_if(1, c)
    rec_i = finish(n_kv + 1)
    for h in range(n_heads):
        lanes = slice(h * LANES, (h + 1) * LANES)
        key_in = room[h:h + 1, :] * jax.nn.sigmoid(-forget_pre[:, lanes].astype(F32))
        high, low = halves(jnp.log1p(-key_in))
        cum = dot_nn(lower, high) + dot_nn(lower, low)
        last = cum[rows - 1:rows, :]
        ecum[:, lanes] = jnp.exp(cum)
        kinv[:, lanes] = (key_in * jnp.exp(-cum)).astype(BF16)
        fresh = (key_in * jnp.exp(last - cum)).astype(BF16)
        st_loc[h] = dot_tn(rec_i[:, lanes], fresh)
        dec[h] = jnp.broadcast_to(jnp.exp(last), dec.shape[1:])

        @pl.when(jnp.logical_and(sp == 0, has_next))
        def _(h=h):
            st_out[h] = st_loc[h].astype(BF16)
            st_copy(h).start()

    hand_on_if(2, 0)
    hand_on_if(2, 1)

    qbuf[...] = finish(n_kv + 2)
    later = jnp.where(iota_r > iota_c, 1.0, 0.0).astype(BF16)
    sums = jnp.concatenate([later, jnp.ones((rows, LANES), BF16)], axis=1)
    scale = 1.0 / math.sqrt(LANES)

    g_heads = n_heads // GROUPS

    def attend(slot, g, diagonal):
        for h in range(g * g_heads, (g + 1) * g_heads):
            lanes = slice(h * LANES, (h + 1) * LANES)
            inner = slice((h - g * g_heads) * LANES, (h - g * g_heads + 1) * LANES)
            z = dot_nt(qbuf[:, lanes], kv[slot, 2 * g, :, inner]) * scale + offs[h]
            keep = -(jnp.maximum(z, 0.0) + jnp.log1p(jnp.exp(-jnp.abs(z))))
            log_stick = z + keep
            if diagonal:
                keep = jnp.where(strict, keep, 0.0)
            high, low = halves(keep)
            both = dot_nn(high, sums) + dot_nn(low, sums)
            stick = jnp.exp(log_stick + both[:, :rows])
            if diagonal:
                stick = jnp.where(strict, stick, 0.0)
            value = dot_nn(stick.astype(BF16), kv[slot, 2 * g + 1, :, inner])
            if diagonal:
                att[:, lanes] = value
                run[h] = both[:, rows:]
            else:
                past = run[h]
                att[:, lanes] += value * jnp.exp(past)
                run[h] = past + both[:, rows:]

    def attend_if(step):
        if step < n_sp:
            @pl.when(sp >= step)
            def _():
                for g in range(GROUPS):
                    attend(sp - step, g, False)

    for g in range(GROUPS):
        attend(sp, g, True)
    for c in range(2, n_kv):
        hand_on_if(2, c)
    attend_if(1)
    rec_q = finish(n_kv + 3)
    for h in range(n_heads):
        lanes = slice(h * LANES, (h + 1) * LANES)
        decayed = (rec_q[:, lanes].astype(F32) * ecum[:, lanes]).astype(BF16)
        qdec[:, lanes] = decayed
        scores = jnp.where(causal, dot_nt(decayed, kinv[:, lanes]), 0.0)
        loc[:, lanes] = dot_nn(scores.astype(BF16), rec_i[:, lanes])

    attend_if(2)

    def block(step, carry):
        for c in range(n_kv):
            hand_on(step, c)
        for g in range(GROUPS):
            attend(sp - step, g, False)
        return carry

    lax.fori_loop(3, sp, block, 0)

    n_head_units = GROUPS + n_heads

    def h_copy(df, c):
        index = (df - 1) * n_head_units + c
        if c < GROUPS:
            lanes = pl.ds(c * g_cols, g_cols)
            source, target = heads.at[0, :, lanes], hrecv.at[df - 1, 0, :, lanes]
        else:
            lanes = pl.ds((c - GROUPS) * LANES, LANES)
            source, target = heads.at[1, :, lanes], hrecv.at[df - 1, 1, :, lanes]
        return pltpu.make_async_remote_copy(
            src_ref=source, dst_ref=target, send_sem=h_send.at[index], recv_sem=h_recv.at[index],
            device_id={"fs": fs_at(df)}, device_id_type=MESH,
        )

    for g in range(GROUPS):
        @pl.when(sp >= 3)
        def _(g=g):
            for c in (2 * g, 2 * g + 1):
                hand_on(sp, c)
            attend(0, g, False)

        cut = slice(g * g_cols, (g + 1) * g_cols)
        heads[0, :, cut] = att[:, cut].astype(BF16)
        for df in range(1, n_fs):
            h_copy(df, g).start()

    for h in range(n_heads):
        lanes = slice(h * LANES, (h + 1) * LANES)

        @pl.when(has_prev)
        def _(h=h, lanes=lanes):
            st_copy(h).wait_recv()

            @pl.when(has_next)
            def _():
                st_out[h] = (st_in[h].astype(F32) * dec[h, 0:1, :] + st_loc[h]).astype(BF16)
                st_copy(h).start()

            loc[:, lanes] += dot_nt(qdec[:, lanes], st_in[h])

        raw = loc[:, lanes]
        norm = lax.rsqrt(jnp.mean(raw * raw, axis=1, keepdims=True) + norm_eps)
        heads[1, :, lanes] = (raw * norm * out_gain[...]).astype(BF16)
        for df in range(1, n_fs):
            h_copy(df, GROUPS + h).start()

    w_copies[N_PROJ].wait()
    w_copies[N_PROJ + 1].wait()

    half = out_cols // CHUNKS

    def pp_copy(df, dt, k):
        index = (df * (n_tp - 1) + dt - 1) * CHUNKS + k
        start = pl.multiple_of(tp_at(dt) * share, share)
        return pltpu.make_async_remote_copy(
            src_ref=part.at[df, k, pl.ds(start, share)], dst_ref=precv2.at[dt - 1, df, k],
            send_sem=pp_send.at[index], recv_sem=pp_recv.at[index],
            device_id={"tp": tp_at(dt)}, device_id_type=MESH,
        )

    def m_copy(df, k):
        index = (df - 1) * CHUNKS + k
        return pltpu.make_async_remote_copy(
            src_ref=mix.at[df - 1, k], dst_ref=mrecv.at[df - 1, k],
            send_sem=m_send.at[index], recv_sem=m_recv.at[index],
            device_id={"fs": fs_at(df)}, device_id_type=MESH,
        )

    def reduced(df, k):
        value = part[df, k, pl.ds(pl.multiple_of(tp * share, share), share)].astype(F32)
        for dt in range(1, n_tp):
            pp_copy(df, dt, k).wait_recv()
            value = value + precv2[dt - 1, df, k].astype(F32)
        return value.astype(BF16)

    def columns(owner, k):
        return pl.ds(pl.multiple_of(owner * out_cols + k * half, LANES), half)

    for df in range(1, n_fs):
        for g in range(GROUPS):
            h_copy(df, g).wait_recv()
        for k in range(CHUNKS):
            part_acc[df - 1, k] = dot_nn(hrecv[df - 1, 0], obuf[0, :, k * half:(k + 1) * half])
    for k in range(CHUNKS):
        cut = slice(k * half, (k + 1) * half)
        part[0, k] = (dot_nn(heads[0], obuf[0, :, cut]) + dot_nn(heads[1], obuf[1, :, cut])).astype(BF16)
        for dt in range(1, n_tp):
            pp_copy(0, dt, k).start()
    for df in range(1, n_fs):
        for h in range(n_heads):
            h_copy(df, GROUPS + h).wait_recv()
        for k in range(CHUNKS):
            cut = slice(k * half, (k + 1) * half)
            part[df, k] = (part_acc[df - 1, k] + dot_nn(hrecv[df - 1, 1], obuf[1, :, cut])).astype(BF16)
            for dt in range(1, n_tp):
                pp_copy(df, dt, k).start()
    for df in range(1, n_fs):
        for k in range(CHUNKS):
            mix[df - 1, k] = reduced(df, k)
            m_copy(df, k).start()
    for k in range(CHUNKS):
        out[:, columns(fs, k)] = reduced(0, k)
    for df in range(1, n_fs):
        source = lax.rem(fs + n_fs - df, n_fs)
        for k in range(CHUNKS):
            m_copy(df, k).wait_recv()
            out[:, columns(source, k)] = mrecv[df - 1, k]

    for df, dt in x_order:
        @pl.when(holder(fs_at(df)) == tp)
        def _(df=df, dt=dt):
            x_copy(df, dt).wait_send()
    for dt in range(1, n_tp):
        ss_copy(dt).wait_send()
        for df in range(1, n_fs):
            f_copy(df, dt).wait_send()
    for df in range(1, n_fs):
        for dt in range(n_tp):
            first_copy(df, dt).wait_send()
        for u in range(1, n_units):
            p_copy(df, u).wait_send()
        for c in range(n_head_units):
            h_copy(df, c).wait_send()
    for k in range(CHUNKS):
        for df in range(1, n_fs):
            m_copy(df, k).wait_send()
        for df in range(n_fs):
            for dt in range(1, n_tp):
                pp_copy(df, dt, k).wait_send()

    @pl.when(has_next)
    def _():
        for h in range(n_heads):
            st_copy(h).wait_send()

        def drain(slot, carry):
            for c in range(n_kv):
                kv_copy(slot, c).wait_send()
            return carry

        lax.fori_loop(0, sp + 1, drain, 0)


def body(
    tokens, mix_gain, attn_query, attn_key, attn_value, rec_query, rec_forget, rec_input,
    break_offset, forget_room, out_gain, out_attn, out_rec,
):
    n_sp, n_fs, n_tp = lax.axis_size("sp"), lax.axis_size("fs"), lax.axis_size("tp")
    rows, feat_t = tokens.shape[1], tokens.shape[2]
    feat_f, cols = attn_query.shape
    width = feat_t * n_tp
    n_heads = cols // LANES
    out_rows, out_cols = out_attn.shape
    share = rows // n_tp
    piece = out_cols // CHUNKS
    n_units = 2 * GROUPS + N_PROJ - 2
    vmem = pl.BlockSpec(memory_space=pltpu.VMEM)
    smem = pl.BlockSpec(memory_space=pltpu.SMEM)
    hbm = pl.BlockSpec(memory_space=pl.ANY)
    dma = pltpu.SemaphoreType.DMA
    square = (n_heads, LANES, LANES)
    result = pl.pallas_call(
        functools.partial(kernel, n_sp, n_fs, n_tp),
        out_shape=jax.ShapeDtypeStruct((share, width), BF16),
        in_specs=[hbm, vmem] + [hbm] * 6 + [smem, vmem, vmem, hbm, hbm],
        out_specs=vmem,
        scratch_shapes=[
            pltpu.VMEM((rows, feat_t), BF16),
            pltpu.VMEM((N_PROJ, feat_f, cols), BF16),
            pltpu.VMEM((2, out_rows, out_cols), BF16),
            pltpu.VMEM((n_fs, rows, feat_f), BF16),
            pltpu.VMEM((n_fs, rows, feat_f), BF16),
            pltpu.VMEM((n_tp, rows, LANES), F32),
            pltpu.VMEM((N_PROJ, rows, cols), F32),
            pltpu.VMEM((n_fs - 1, N_PROJ, rows, cols), BF16),
            pltpu.VMEM((n_fs - 1, N_PROJ, rows, cols), BF16),
            pltpu.VMEM((n_sp, 2 * GROUPS, rows, cols // GROUPS), BF16),
            pltpu.VMEM((rows, cols), BF16),
            pltpu.VMEM((rows, cols), BF16),
            pltpu.VMEM((rows, cols), F32),
            pltpu.VMEM((rows, cols), BF16),
            pltpu.VMEM((rows, cols), F32),
            pltpu.VMEM((n_heads, rows, LANES), F32),
            pltpu.VMEM((rows, cols), F32),
            pltpu.VMEM(square, F32),
            pltpu.VMEM((n_heads, 8, LANES), F32),
            pltpu.VMEM(square, BF16),
            pltpu.VMEM(square, BF16),
            pltpu.VMEM((2, rows, cols), BF16),
            pltpu.VMEM((n_fs - 1, 2, rows, cols), BF16),
            pltpu.VMEM((n_fs - 1, CHUNKS, rows, piece), F32),
            pltpu.VMEM((n_fs, CHUNKS, rows, piece), BF16),
            pltpu.VMEM((n_tp - 1, n_fs, CHUNKS, share, piece), BF16),
            pltpu.VMEM((n_fs - 1, CHUNKS, share, piece), BF16),
            pltpu.VMEM((n_fs - 1, CHUNKS, share, piece), BF16),
            dma((1,)), dma((N_PROJ + 2,)),
            dma((n_fs * n_tp,)), dma((n_fs * n_tp,)), dma((n_fs * n_tp,)),
            dma((n_tp - 1,)), dma((n_tp,)),
            dma(((n_fs - 1) * (n_units + n_tp),)), dma(((n_fs - 1) * (n_units + n_tp),)),
            dma((n_sp * 2 * GROUPS,)), dma((n_sp * 2 * GROUPS,)),
            dma((2 * n_heads,)),
            dma(((n_fs - 1) * (GROUPS + n_heads),)), dma(((n_fs - 1) * (GROUPS + n_heads),)),
            dma((n_fs * (n_tp - 1) * CHUNKS,)), dma((n_fs * (n_tp - 1) * CHUNKS,)),
            dma(((n_fs - 1) * CHUNKS,)), dma(((n_fs - 1) * CHUNKS,)),
        ],
        compiler_params=pltpu.CompilerParams(
            collective_id=0, has_side_effects=True, vmem_limit_bytes=60 * 1024 * 1024
        ),
        name="layer",
    )(
        tokens.reshape(rows, feat_t), mix_gain.reshape(1, width),
        attn_key, attn_value, rec_forget, rec_input, attn_query, rec_query,
        break_offset, forget_room, out_gain.reshape(1, LANES), out_attn, out_rec,
    )
    return result.reshape(1, share, width)


def solution(mesh):
    placed = (
        P(("grp", "fs"), "sp", "tp"),
        P(),
        P("fs", "tp"),
        P("fs", "tp"),
        P("fs", "tp"),
        P("fs", "tp"),
        P("fs", "tp"),
        P("fs", "tp"),
        P("tp"),
        P("tp", None),
        P(),
        P("tp", "fs"),
        P("tp", "fs"),
    )
    return jax.shard_map(
        body,
        mesh=mesh,
        in_specs=placed,
        out_specs=P(("grp", "fs"), ("sp", "tp"), None),
        check_vma=False,
    )
```

profile of v0, /device:TPU:26, one launch (start us, length us, event | category | flops | bytes accessed | tf_op | source)
XLA Modules:
  0.0 46.6 jit_solution(1768195455901803233)
XLA Ops:
  0.0 44.9 %layer.1 = bf16[64,2048]{1,0:T(8,128)(2,1)} custom-call(bf16[128,1024]{1,0:T(8,128)(2,1)} %bitcast.5, f32[1,2048]{1,0:T(1,128)} %bitcast.6, bf16[1024,512]{1,0:T(8,128)(2,1)} %w_k.1, bf16[1024,512]{1,0:T(8,128)(2,1)} %w_v.1, bf16[1024,512]{1,0:T(8,128)(2,1)} %w_f.1, bf16[1024,512]{1,0:T(8,128)(2,1)} %w_i.1, bf16[1024,512]{1,0:T(8,128)(2,1)} %w_q.1, ...), custom_call_target="tpu_custom_call" | custom-call | tf_op jit(solution)/shard_map/layer/pallas_call | solution.py:541
  44.9 1.7 %copy.15 = bf16[1,64,2048]{2,1,0:T(8,128)(2,1)} copy(bf16[1,64,2048]{2,1,0:T(8,128)(2,1)} %bitcast.4) | data formatting | bytes 524288
where the time goes:
time: 47.2 us; the launch traced here: 46.6 us
  Pallas kernels  44.9 us (95%)
  local copies, waits for them, and re-layouts  1.67 us (4%)
    pallas_call x1, Pallas kernels, body(): pl.pallas_call(functools.partial(kernel, n_sp, n_fs, n_tp), out_shape=jax...  44.9 us
    unnamed x1, local copies, waits for them, and re-layouts  1.67 us

commit v1 on v0

--- a/solution.py
+++ b/solution.py
@@ -37,11 +37,12 @@
 
 def kernel(
     n_sp, n_fs, n_tp,
-    tok_hbm, gain, w_k, w_v, w_f, w_i, w_q, w_r, offs, room, out_gain, o_attn, o_rec,
+    tok_hbm, gain_hbm, w_k, w_v, w_f, w_i, w_q, w_r, offs_hbm, room_hbm, out_gain_hbm, o_attn, o_rec,
     out,
+    gain, offs, room, out_gain,
     tok, wbuf, obuf, xt, xg, ss, acc, psend, precv, kv, qbuf, qdec, ecum, kinv,
     att, run, loc, st_loc, dec, st_in, st_out, heads, hrecv, part_acc, part, precv2, mix, mrecv,
-    t_sem, w_sem, x_send, x_recv, f_send, ss_send, ss_recv, p_send, p_recv, kv_send, kv_recv,
+    t_sem, s_sem, w_sem, x_send, x_recv, f_send, ss_send, ss_recv, p_send, p_recv, kv_send, kv_recv,
     st_sem, h_send, h_recv, pp_send, pp_recv, m_send, m_recv,
 ):
     sp, fs, tp = lax.axis_index("sp"), lax.axis_index("fs"), lax.axis_index("tp")
@@ -63,6 +64,14 @@
 
     tok_copy = pltpu.make_async_copy(tok_hbm, tok, t_sem.at[0])
     tok_copy.start()
+    small_copies = [
+        pltpu.make_async_copy(source, target, s_sem.at[i])
+        for i, (source, target) in enumerate(
+            ((gain_hbm, gain), (offs_hbm, offs), (room_hbm, room), (out_gain_hbm, out_gain))
+        )
+    ]
+    for copy in small_copies:
+        copy.start()
     w_copies = [
         pltpu.make_async_copy(w, wbuf.at[i], w_sem.at[i])
         for i, w in enumerate((w_k, w_v, w_f, w_i, w_q, w_r))
@@ -148,6 +157,8 @@
         ss_copy(dt).start()
 
     own_holder = holder(fs) == tp
+    for copy in small_copies:
+        copy.wait()
     gain_f = gain[:, pl.ds(pl.multiple_of(fs * feat_f, LANES), feat_f)]
 
     @pl.when(own_holder)
@@ -326,7 +337,7 @@
         for h in range(g * g_heads, (g + 1) * g_heads):
             lanes = slice(h * LANES, (h + 1) * LANES)
             inner = slice((h - g * g_heads) * LANES, (h - g * g_heads + 1) * LANES)
-            z = dot_nt(qbuf[:, lanes], kv[slot, 2 * g, :, inner]) * scale + offs[h]
+            z = dot_nt(qbuf[:, lanes], kv[slot, 2 * g, :, inner]) * scale + offs[0:1, h:h + 1]
             keep = -(jnp.maximum(z, 0.0) + jnp.log1p(jnp.exp(-jnp.abs(z))))
             log_stick = z + keep
             if diagonal:
@@ -534,16 +545,19 @@
     piece = out_cols // CHUNKS
     n_units = 2 * GROUPS + N_PROJ - 2
     vmem = pl.BlockSpec(memory_space=pltpu.VMEM)
-    smem = pl.BlockSpec(memory_space=pltpu.SMEM)
     hbm = pl.BlockSpec(memory_space=pl.ANY)
     dma = pltpu.SemaphoreType.DMA
     square = (n_heads, LANES, LANES)
     result = pl.pallas_call(
         functools.partial(kernel, n_sp, n_fs, n_tp),
-        out_shape=jax.ShapeDtypeStruct((share, width), BF16),
-        in_specs=[hbm, vmem] + [hbm] * 6 + [smem, vmem, vmem, hbm, hbm],
+        out_shape=pltpu.VMEM((share, width), BF16),
+        in_specs=[hbm] * 13,
         out_specs=vmem,
         scratch_shapes=[
+            pltpu.VMEM((1, width), F32),
+            pltpu.VMEM((1, n_heads), F32),
+            pltpu.VMEM((n_heads, LANES), F32),
+            pltpu.VMEM((1, LANES), F32),
             pltpu.VMEM((rows, feat_t), BF16),
             pltpu.VMEM((N_PROJ, feat_f, cols), BF16),
             pltpu.VMEM((2, out_rows, out_cols), BF16),
@@ -572,7 +586,7 @@
             pltpu.VMEM((n_tp - 1, n_fs, CHUNKS, share, piece), BF16),
             pltpu.VMEM((n_fs - 1, CHUNKS, share, piece), BF16),
             pltpu.VMEM((n_fs - 1, CHUNKS, share, piece), BF16),
-            dma((1,)), dma((N_PROJ + 2,)),
+            dma((1,)), dma((4,)), dma((N_PROJ + 2,)),
             dma((n_fs * n_tp,)), dma((n_fs * n_tp,)), dma((n_fs * n_tp,)),
             dma((n_tp - 1,)), dma((n_tp,)),
             dma(((n_fs - 1) * (n_units + n_tp),)), dma(((n_fs - 1) * (n_units + n_tp),)),
@@ -589,7 +603,7 @@
     )(
         tokens.reshape(rows, feat_t), mix_gain.reshape(1, width),
         attn_key, attn_value, rec_forget, rec_input, attn_query, rec_query,
-        break_offset, forget_room, out_gain.reshape(1, LANES), out_attn, out_rec,
+        break_offset.reshape(1, n_heads), forget_room, out_gain.reshape(1, LANES), out_attn, out_rec,
     )
     return result.reshape(1, share, width)
 

time: 47.2 us -> 44.8 us (0.949)
  Pallas kernels: 44.9 us -> 43.5 us
  local copies, waits for them, and re-layouts: 1.67 us -> 0.71 us
    pallas_call x1, Pallas kernels: 44.9 us -> 43.5 us  [body(): pl.pallas_call(functools.partial(kernel, n_sp, n_fs, n_tp), out_shape=plt...]
    unnamed x1, local copies, waits for them, and re-layouts: 1.67 us -> 0.71 us
where the time goes in v1:
time: 44.8 us; the launch traced here: 44.2 us
  Pallas kernels  43.5 us (97%)
  local copies, waits for them, and re-layouts  0.71 us (2%)
    pallas_call x1, Pallas kernels, body(): pl.pallas_call(functools.partial(kernel, n_sp, n_fs, n_tp), out_shape=plt...  43.5 us

profile of v1, /device:TPU:26, one launch (start us, length us, event | category | flops | bytes accessed | tf_op | source)
XLA Modules:
  0.0 44.2 jit_solution(433895050036966005)
XLA Ops:
  0.0 43.5 %layer.1 = bf16[64,2048]{1,0:T(8,128)(2,1)S(1)} custom-call(bf16[128,1024]{1,0:T(8,128)(2,1)} %bitcast.6, f32[1,2048]{1,0:T(1,128)} %bitcast.7, bf16[1024,512]{1,0:T(8,128)(2,1)} %w_k.1, bf16[1024,512]{1,0:T(8,128)(2,1)} %w_v.1, bf16[1024,512]{1,0:T(8,128)(2,1)} %w_f.1, bf16[1024,512]{1,0:T(8,128)(2,1)} %w_i.1, bf16[1024,512]{1,0:T(8,128)(2,1)} %w_q.1, ...), custom_call_target="tpu_custom_call" | custom-call | tf_op jit(solution)/shard_map/layer/pallas_call | solution.py:551
  43.5 0.7 %copy.15 = bf16[1,64,2048]{2,1,0:T(8,128)(2,1)} copy(bf16[1,64,2048]{2,1,0:T(8,128)(2,1)S(1)} %bitcast.5) | data formatting | bytes 524288

commit v2 on v1

v2 whole, which is shorter than its diff:
```python
import functools
import math

import jax
import jax.numpy as jnp
from jax import lax
from jax.experimental import pallas as pl
from jax.experimental.pallas import tpu as pltpu
from jax.sharding import PartitionSpec as P

LANES = 128
norm_eps = 1e-06
MESH = pl.DeviceIdType.MESH
F32 = jnp.float32
BF16 = jnp.bfloat16
N_PROJ = 6
KEY, VALUE, FORGET, INPUT, QUERY, READ = range(N_PROJ)
GROUPS = 2
CHUNKS = 2
X_CHUNKS = 4
N_SMALL = 4


def dot_nn(a, b):
    return lax.dot_general(a, b, (((1,), (0,)), ((), ())), preferred_element_type=F32)


def dot_nt(a, b):
    return lax.dot_general(a, b, (((1,), (1,)), ((), ())), preferred_element_type=F32)


def dot_tn(a, b):
    return lax.dot_general(a, b, (((0,), (0,)), ((), ())), preferred_element_type=F32)


def halves(x):
    high = x.astype(BF16)
    return high, (x - high.astype(F32)).astype(BF16)


def unit_list(cols):
    g_cols = cols // GROUPS
    units = [(w, 0) for w in (FORGET, INPUT)]
    for g in range(1, GROUPS):
        units += [(w, g * g_cols) for w in (KEY, VALUE, FORGET, INPUT)]
    units += [(w, g * g_cols) for w in (QUERY, READ) for g in range(GROUPS)]
    return units


def kernel(
    n_sp, n_fs, n_tp,
    tok_hbm, gain_hbm, w_k, w_v, w_f, w_i, w_q, w_r, offs_hbm, room_hbm, out_gain_hbm, o_attn, o_rec,
    out,
    gain, offs, room, out_gain,
    tok, wbuf, obuf, xt, xg, ss, acc, psend, precv, kv, qbuf, qdec, ecum, kinv, fresh, rec_i,
    att, run, loc, st_loc, dec, st_in, st_out, heads, hrecv, part_acc, mix, mrecv,
    t_sem, s_sem, w_sem, x_send, x_recv, f_send, own_send, own_recv, ss_send, ss_recv, p_send, p_recv,
    kv_send, kv_recv, st_send, st_recv, o_send, o_recv, h_send, h_recv, m_send, m_recv,
):
    sp, fs, tp = lax.axis_index("sp"), lax.axis_index("fs"), lax.axis_index("tp")
    rows, feat_t = tok.shape
    feat_f = xt.shape[2]
    width = feat_t * n_tp
    cols = wbuf.shape[2]
    n_heads = cols // LANES
    share = rows // n_tp
    out_cols = obuf.shape[3]
    g_cols = cols // GROUPS
    g_heads = n_heads // GROUPS
    n_kv = X_CHUNKS + 2 * (GROUPS - 1)
    x_rows = rows // X_CHUNKS
    relay = 0
    is_relay = tp == relay
    has_next = sp < n_sp - 1
    has_prev = sp > 0

    def fs_at(step):
        return lax.rem(fs + step, n_fs)

    def tp_at(step):
        return lax.rem(tp + step, n_tp)

    def group(g):
        return slice(g * g_cols, (g + 1) * g_cols)

    tok_copy = pltpu.make_async_copy(tok_hbm, tok, t_sem.at[0])
    tok_copy.start()
    barrier = pltpu.get_barrier_semaphore()
    for df in range(n_fs):
        for dt in range(n_tp):
            if df or dt:
                pl.semaphore_signal(
                    barrier, inc=1, device_id={"fs": fs_at(df), "tp": tp_at(dt)}, device_id_type=MESH
                )

    @pl.when(has_next)
    def _():
        pl.semaphore_signal(barrier, inc=1, device_id={"sp": sp + 1}, device_id_type=MESH)

    @pl.when(has_prev)
    def _():
        pl.semaphore_signal(barrier, inc=1, device_id={"sp": sp - 1}, device_id_type=MESH)

    small_copies = [
        pltpu.make_async_copy(source, target, s_sem.at[i])
        for i, (source, target) in enumerate(
            ((gain_hbm, gain), (offs_hbm, offs), (room_hbm, room), (out_gain_hbm, out_gain))
        )
    ]
    w_copies = [
        pltpu.make_async_copy(w, wbuf.at[i], w_sem.at[i])
        for i, w in enumerate((w_k, w_v, w_f, w_i, w_q, w_r))
    ]
    o_copies = [
        pltpu.make_async_copy(w, obuf.at[tp, i], w_sem.at[N_PROJ + i]) for i, w in enumerate((o_attn, o_rec))
    ]
    for copy in small_copies + w_copies + o_copies:
        copy.start()
    tok_copy.wait()

    next_count = jnp.where(has_next, 1, 0)
    prev_count = jnp.where(has_prev, 1, 0)
    pl.semaphore_wait(barrier, n_fs * n_tp - 1 + next_count + prev_count)

    def holder(f_index):
        return (f_index * feat_f) // feat_t

    def held(f_index):
        return pl.ds(pl.multiple_of(lax.rem(f_index * feat_f, feat_t), LANES), feat_f)

    def x_part(c):
        return pl.ds(c * x_rows, x_rows)

    def x_copy(df, c):
        return pltpu.make_async_remote_copy(
            src_ref=tok.at[x_part(c), held(fs_at(df))], dst_ref=xt.at[fs, x_part(c)],
            send_sem=x_send.at[(df - 1) * X_CHUNKS + c], recv_sem=x_recv.at[fs * X_CHUNKS + c],
            device_id={"fs": fs_at(df), "tp": relay}, device_id_type=MESH,
        )

    def f_copy(df, c, dt):
        slot = fs_at(df)
        return pltpu.make_async_remote_copy(
            src_ref=xt.at[slot, x_part(c)], dst_ref=xt.at[slot, x_part(c)],
            send_sem=f_send.at[((df - 1) * X_CHUNKS + c) * (n_tp - 1) + dt - 1],
            recv_sem=x_recv.at[slot * X_CHUNKS + c],
            device_id={"tp": tp_at(dt)}, device_id_type=MESH,
        )

    def own_copy(dt):
        return pltpu.make_async_remote_copy(
            src_ref=tok.at[:, held(fs)], dst_ref=xt.at[fs],
            send_sem=own_send.at[dt - 1], recv_sem=own_recv.at[0],
            device_id={"tp": tp_at(dt)}, device_id_type=MESH,
        )

    for df in range(1, n_fs):
        @pl.when(holder(fs_at(df)) == tp)
        def _(df=df):
            for c in range(X_CHUNKS):
                x_copy(df, c).start()

    own_holder = holder(fs) == tp

    @pl.when(own_holder)
    def _():
        for dt in range(1, n_tp):
            own_copy(dt).start()

    squares = jnp.zeros((rows, LANES), F32)
    for c in range(feat_t // LANES):
        piece = tok[:, c * LANES:(c + 1) * LANES].astype(F32)
        squares = squares + piece * piece
    ss[tp] = squares

    def ss_copy(dt):
        return pltpu.make_async_remote_copy(
            src_ref=ss.at[tp], dst_ref=ss.at[tp],
            send_sem=ss_send.at[dt - 1], recv_sem=ss_recv.at[tp],
            device_id={"tp": tp_at(dt)}, device_id_type=MESH,
        )

    for dt in range(1, n_tp):
        ss_copy(dt).start()

    for copy in small_copies:
        copy.wait()
    gain_f = gain[:, pl.ds(pl.multiple_of(fs * feat_f, LANES), feat_f)]

    @pl.when(own_holder)
    def _():
        xg[0] = (tok[:, held(fs)].astype(F32) * gain_f).astype(BF16)

    units = unit_list(cols)
    n_units = len(units)

    def first_copy(df, c):
        index = (df - 1) * (n_units + X_CHUNKS) + n_units + c
        return pltpu.make_async_remote_copy(
            src_ref=psend.at[df - 1, pl.ds(KEY, 2), x_part(c), pl.ds(0, g_cols)],
            dst_ref=precv.at[df - 1, pl.ds(KEY, 2), x_part(c), pl.ds(0, g_cols)],
            send_sem=p_send.at[index], recv_sem=p_recv.at[index],
            device_id={"fs": fs_at(df)}, device_id_type=MESH,
        )

    def p_copy(df, u):
        w, first = units[u]
        index = (df - 1) * (n_units + X_CHUNKS) + u
        return pltpu.make_async_remote_copy(
            src_ref=psend.at[df - 1, w, :, pl.ds(first, g_cols)],
            dst_ref=precv.at[df - 1, w, :, pl.ds(first, g_cols)],
            send_sem=p_send.at[index], recv_sem=p_recv.at[index],
            device_id={"fs": fs_at(df)}, device_id_type=MESH,
        )

    @pl.when(jnp.logical_not(own_holder))
    def _():
        pltpu.make_async_remote_copy(
            src_ref=xt.at[fs], dst_ref=xt.at[fs], send_sem=own_send.at[0], recv_sem=own_recv.at[0],
            device_id={"tp": tp_at(1)}, device_id_type=MESH,
        ).wait_recv()
        xg[0] = (xt[fs].astype(F32) * gain_f).astype(BF16)

    total = ss[tp]
    for dt in range(1, n_tp):
        other = tp_at(dt)
        pltpu.make_async_remote_copy(
            src_ref=ss.at[other], dst_ref=ss.at[other],
            send_sem=ss_send.at[dt - 1], recv_sem=ss_recv.at[other],
            device_id={"tp": other}, device_id_type=MESH,
        ).wait_recv()
        total = total + ss[other]
    factor = lax.rsqrt(jnp.sum(total, axis=1, keepdims=True) / width + norm_eps)

    def own_product(w, cut):
        acc[w, :, cut] = dot_nn(xg[0], wbuf[w, :, cut])

    w_copies[KEY].wait()
    own_product(KEY, group(0))
    w_copies[VALUE].wait()
    own_product(VALUE, group(0))
    for c in range(X_CHUNKS):
        part = slice(c * x_rows, (c + 1) * x_rows)
        for df in range(1, n_fs):
            slot = fs_at(df)
            view = xt.at[slot, x_part(c)]
            pltpu.make_async_remote_copy(
                src_ref=view, dst_ref=view, send_sem=x_send.at[0], recv_sem=x_recv.at[slot * X_CHUNKS + c],
                device_id={"tp": tp_at(1)}, device_id_type=MESH,
            ).wait_recv()

            @pl.when(is_relay)
            def _(df=df, c=c):
                for dt in range(1, n_tp):
                    f_copy(df, c, dt).start()

            xg[df, part, :] = (xt[slot, part, :].astype(F32) * gain_f).astype(BF16)
            for w in (KEY, VALUE):
                psend[df - 1, w, part, 0:g_cols] = dot_nn(xg[df, part, :], wbuf[w, :, 0:g_cols]).astype(BF16)
            first_copy(df, c).start()

    def partials(w, first, count):
        cut = slice(first, first + count)
        for df in range(1, n_fs):
            psend[df - 1, w, :, cut] = dot_nn(xg[df], wbuf[w, :, cut]).astype(BF16)

    def send_unit(w, g):
        for df in range(1, n_fs):
            p_copy(df, units.index((w, g * g_cols))).start()


    def finish(w, g):
        cut = group(g)
        value = acc[w, :, cut]
        for df in range(1, n_fs):
            p_copy(df, units.index((w, g * g_cols))).wait_recv()
            value = value + precv[df - 1, w, :, cut].astype(F32)
        return (value * factor).astype(BF16)

    def kv_copy(slot, c):
        if c < X_CHUNKS:
            view = kv.at[slot, pl.ds(0, 2), x_part(c)]
        else:
            view = kv.at[slot, 2 + c - X_CHUNKS]
        return pltpu.make_async_remote_copy(
            src_ref=view, dst_ref=view,
            send_sem=kv_send.at[slot * n_kv + c], recv_sem=kv_recv.at[slot * n_kv + c],
            device_id={"sp": lax.rem(sp + 1, n_sp)}, device_id_type=MESH,
        )

    def group_kv(g):
        if g == 0:
            return range(X_CHUNKS)
        return range(X_CHUNKS + 2 * (g - 1), X_CHUNKS + 2 * g)

    def send_kv(c):
        @pl.when(has_next)
        def _():
            kv_copy(sp, c).start()

    def finish_first(c):
        part = slice(c * x_rows, (c + 1) * x_rows)
        for df in range(1, n_fs):
            first_copy(df, c).wait_recv()
        for w in (KEY, VALUE):
            value = acc[w, part, 0:g_cols]
            for df in range(1, n_fs):
                value = value + precv[df - 1, w, part, 0:g_cols].astype(F32)
            kv[sp, w, part, :] = (value * factor[part]).astype(BF16)
        send_kv(c)

    def finish_kv(w, g):
        kv[sp, 2 * g + w] = finish(w, g)
        send_kv(X_CHUNKS + 2 * (g - 1) + w)

    def hand_on(step, c):
        kv_copy(sp - step, c).wait_recv()

        @pl.when(has_next)
        def _():
            kv_copy(sp - step, c).start()

    def hand_on_if(step, c):
        if step < n_sp:
            pl.when(sp >= step)(functools.partial(hand_on, step, c))

    for w in (FORGET, INPUT):
        w_copies[w].wait()
        partials(w, 0, cols)
        send_unit(w, 0)
        finish_first(w - FORGET)
    for w in (KEY, VALUE):
        partials(w, g_cols, cols - g_cols)
        for g in range(1, GROUPS):
            send_unit(w, g)
        finish_first(2 + w)
    for c in range(4, X_CHUNKS):
        finish_first(c)
    for w in (FORGET, INPUT):
        for g in range(1, GROUPS):
            send_unit(w, g)
    for w in (QUERY, READ):
        w_copies[w].wait()
        partials(w, 0, cols)
        for g in range(GROUPS):
            send_unit(w, g)
    for w in (FORGET, INPUT):
        own_product(w, slice(0, cols))
    for w in (KEY, VALUE):
        own_product(w, slice(g_cols, cols))
    for w in (QUERY, READ):
        own_product(w, slice(0, cols))

    def o_copy(dt):
        return pltpu.make_async_remote_copy(
            src_ref=obuf.at[tp], dst_ref=obuf.at[tp], send_sem=o_send.at[dt - 1], recv_sem=o_recv.at[tp],
            device_id={"tp": tp_at(dt)}, device_id_type=MESH,
        )

    for copy in o_copies:
        copy.wait()
    for dt in range(1, n_tp):
        o_copy(dt).start()

    iota_r = lax.broadcasted_iota(jnp.int32, (rows, rows), 0)
    iota_c = lax.broadcasted_iota(jnp.int32, (rows, rows), 1)
    causal = iota_r >= iota_c
    strict = jnp.concatenate([iota_c < iota_r] * g_heads, axis=0)
    lower = jnp.where(causal, 1.0, 0.0).astype(BF16)
    lower = jnp.concatenate([lower, lower], axis=1)
    later = jnp.where(iota_r > iota_c, 1.0, 0.0).astype(BF16)
    sums = jnp.concatenate([later, jnp.ones((rows, LANES), BF16)], axis=1)
    sums = jnp.concatenate([sums, sums], axis=0)
    scale = 1.0 / math.sqrt(LANES)

    def lanes_of(h):
        return slice(h * LANES, (h + 1) * LANES)

    def heads_of(g):
        return range(g * g_heads, (g + 1) * g_heads)

    def gates(g):
        cut = group(g)
        rooms = jnp.concatenate([room[h:h + 1, :] for h in heads_of(g)], axis=1)
        key_in = rooms * jax.nn.sigmoid(-finish(FORGET, g).astype(F32))
        high, low = halves(jnp.log1p(-key_in))
        cum = dot_nn(lower, jnp.concatenate([high, low], axis=0))
        last = cum[rows - 1:rows, :]
        ecum[:, cut] = jnp.exp(cum)
        kinv[:, cut] = (key_in * jnp.exp(-cum)).astype(BF16)
        fresh[:, cut] = (key_in * jnp.exp(last - cum)).astype(BF16)
        decay = jnp.exp(last)
        for i, h in enumerate(heads_of(g)):
            dec[h] = jnp.broadcast_to(decay[:, lanes_of(i)], dec.shape[1:])

    def st_copy(h):
        return pltpu.make_async_remote_copy(
            src_ref=st_out.at[h], dst_ref=st_in.at[h], send_sem=st_send.at[h], recv_sem=st_recv.at[h],
            device_id={"sp": lax.rem(sp + 1, n_sp)}, device_id_type=MESH,
        )

    def local_state(g):
        rec_i[:, group(g)] = finish(INPUT, g)
        for h in heads_of(g):
            st_loc[h] = dot_tn(rec_i[:, lanes_of(h)], fresh[:, lanes_of(h)])

            @pl.when(jnp.logical_and(sp == 0, has_next))
            def _(h=h):
                st_out[h] = st_loc[h].astype(BF16)
                st_copy(h).start()

    def state_step(g):
        for h in heads_of(g):
            st_copy(h).wait_recv()

            @pl.when(has_next)
            def _(h=h):
                st_out[h] = (st_in[h].astype(F32) * dec[h, 0:1, :] + st_loc[h]).astype(BF16)
                st_copy(h).start()

    def state_step_if(at, g):
        if at < n_sp:
            pl.when(sp == at)(functools.partial(state_step, g))

    def read_local(g):
        cut = group(g)
        qdec[:, cut] = (finish(READ, g).astype(F32) * ecum[:, cut]).astype(BF16)
        for h in heads_of(g):
            lanes = lanes_of(h)
            scores = jnp.where(causal, dot_nt(qdec[:, lanes], kinv[:, lanes]), 0.0)
            loc[:, lanes] = dot_nn(scores.astype(BF16), rec_i[:, lanes])

    n_parts = 2 * GROUPS

    def h_copy(df, dt, kind, g):
        index = ((df * n_tp + dt) * 2 + kind) * GROUPS + g
        lands = (n_tp - dt) % n_tp
        lands_index = ((df * n_tp + lands) * 2 + kind) * GROUPS + g
        return pltpu.make_async_remote_copy(
            src_ref=heads.at[kind, pl.ds(pl.multiple_of(tp_at(dt) * share, share), share), pl.ds(g * g_cols, g_cols)],
            dst_ref=hrecv.at[df, lands, kind, :, pl.ds(g * g_cols, g_cols)],
            send_sem=h_send.at[index], recv_sem=h_recv.at[lands_index],
            device_id={"fs": fs_at(df), "tp": tp_at(dt)}, device_id_type=MESH,
        )

    h_order = [(df, dt) for df in list(range(1, n_fs)) + [0] for dt in range(n_tp) if df or dt]

    def h_wait(df, dt, kind, g):
        view = hrecv.at[df, dt, kind, :, pl.ds(g * g_cols, g_cols)]
        pltpu.make_async_remote_copy(
            src_ref=view, dst_ref=view, send_sem=h_send.at[0],
            recv_sem=h_recv.at[((df * n_tp + dt) * 2 + kind) * GROUPS + g],
            device_id={"tp": tp_at(1)}, device_id_type=MESH,
        ).wait_recv()

    def send_attn(g):
        heads[0, :, group(g)] = att[:, group(g)].astype(BF16)
        for df, dt in h_order:
            h_copy(df, dt, 0, g).start()

    def send_attn_if(condition, g):
        pl.when(condition)(functools.partial(send_attn, g))

    def send_rec(g):
        for h in heads_of(g):
            lanes = lanes_of(h)

            @pl.when(has_prev)
            def _(h=h, lanes=lanes):
                loc[:, lanes] += dot_nt(qdec[:, lanes], st_in[h])

            raw = loc[:, lanes]
            norm = lax.rsqrt(jnp.mean(raw * raw, axis=1, keepdims=True) + norm_eps)
            heads[1, :, lanes] = (raw * norm * out_gain[...]).astype(BF16)
        for df, dt in h_order:
            h_copy(df, dt, 1, g).start()

    def attend(slot, g, diagonal):
        z = jnp.concatenate(
            [
                dot_nt(qbuf[:, lanes_of(h)], kv[slot, 2 * g, :, lanes_of(i)]) * scale + offs[0:1, h:h + 1]
                for i, h in enumerate(heads_of(g))
            ],
            axis=0,
        )
        keep = -(jnp.maximum(z, 0.0) + jnp.log(1.0 + jnp.exp(-jnp.abs(z))))
        log_stick = z + keep
        if diagonal:
            keep = jnp.where(strict, keep, 0.0)
        both = dot_nn(jnp.concatenate(halves(keep), axis=1), sums)
        stick = jnp.exp(log_stick + both[:, :rows])
        if diagonal:
            stick = jnp.where(strict, stick, 0.0)
        stick = stick.astype(BF16)
        for i, h in enumerate(heads_of(g)):
            mine = slice(i * rows, (i + 1) * rows)
            value = dot_nn(stick[mine], kv[slot, 2 * g + 1, :, lanes_of(i)])
            if diagonal:
                att[:, lanes_of(h)] = value
                run[h] = both[mine, rows:]
            else:
                past = run[h]
                att[:, lanes_of(h)] += value * jnp.exp(past)
                run[h] = past + both[mine, rows:]

    def attend_if(step, g):
        if step < n_sp:
            pl.when(sp >= step)(functools.partial(attend, sp - step, g, False))

    def attend_rest(g):
        def block(step, carry):
            for c in group_kv(g):
                hand_on(step, c)
            attend(sp - step, g, False)
            return carry

        lax.fori_loop(3, sp + 1, block, 0)

    near = sp < 3
    far = sp >= 3
    for c in group_kv(0):
        hand_on_if(1, c)
    gates(0)
    local_state(0)
    for c in group_kv(0):
        hand_on_if(2, c)
    for g in range(1, GROUPS):
        for w in (KEY, VALUE):
            finish_kv(w, g)
    state_step_if(1, 0)
    for g in range(1, GROUPS):
        gates(g)
        hand_on_if(1, group_kv(g)[0])
        local_state(g)
        hand_on_if(1, group_kv(g)[1])
    state_step_if(2, 0)
    qbuf[:, group(0)] = finish(QUERY, 0)
    attend(sp, 0, True)
    attend_if(1, 0)
    attend_if(2, 0)
    attend_rest(0)
    send_attn(0)
    for g in range(1, GROUPS):
        hand_on_if(2, group_kv(g)[0])
        state_step_if(1, g)
        qbuf[:, group(g)] = finish(QUERY, g)
        attend(sp, g, True)
        hand_on_if(2, group_kv(g)[1])
    read_local(0)

    @pl.when(far)
    def _():
        state_step(0)

    send_rec(0)
    for g in range(1, GROUPS):
        attend_if(1, g)
        state_step_if(2, g)
        attend_if(2, g)

        @pl.when(near)
        def _(g=g):
            send_attn(g)

        read_local(g)

        @pl.when(near)
        def _(g=g):
            send_rec(g)

        @pl.when(far)
        def _(g=g):
            attend_rest(g)
            send_attn(g)
            state_step(g)
            send_rec(g)

    for dt in range(1, n_tp):
        other = tp_at(dt)
        pltpu.make_async_remote_copy(
            src_ref=obuf.at[other], dst_ref=obuf.at[other], send_sem=o_send.at[dt - 1], recv_sem=o_recv.at[other],
            device_id={"tp": other}, device_id_type=MESH,
        ).wait_recv()

    half = out_cols // CHUNKS

    def m_copy(df, k):
        index = (df - 1) * CHUNKS + k
        return pltpu.make_async_remote_copy(
            src_ref=mix.at[df - 1, k], dst_ref=mrecv.at[df - 1, k],
            send_sem=m_send.at[index], recv_sem=m_recv.at[index],
            device_id={"fs": fs_at(n_fs - df)}, device_id_type=MESH,
        )

    def columns(owner, k):
        return pl.ds(pl.multiple_of(owner * out_cols + k * half, LANES), half)

    def product(df, kind, g, cut):
        value = None
        for dt in range(n_tp):
            if df == 0 and dt == 0:
                left = heads[kind, pl.ds(pl.multiple_of(tp * share, share), share), group(g)]
            else:
                left = hrecv[df, dt, kind, :, group(g)]
            term = dot_nn(left, obuf[tp_at(dt), kind, group(g), cut])
            value = term if value is None else value + term
        return value

    whole = slice(0, out_cols)
    pieces = [(kind, g) for g in range(GROUPS) for kind in range(2)]
    for df in range(1, n_fs):
        for place, (kind, g) in enumerate(pieces[:-1]):
            for dt in range(n_tp):
                h_wait(df, dt, kind, g)
            if place == 0:
                part_acc[df - 1] = product(df, kind, g, whole)
            else:
                part_acc[df - 1] += product(df, kind, g, whole)
    for df in range(1, n_fs):
        kind, g = pieces[-1]
        for dt in range(n_tp):
            h_wait(df, dt, kind, g)
        for k in range(CHUNKS):
            cut = slice(k * half, (k + 1) * half)
            mix[df - 1, k] = (part_acc[df - 1, :, cut] + product(df, kind, g, cut)).astype(BF16)
            m_copy(df, k).start()
    for dt in range(1, n_tp):
        for kind in range(2):
            for g in range(GROUPS):
                h_wait(0, dt, kind, g)
    for k in range(CHUNKS):
        cut = slice(k * half, (k + 1) * half)
        value = None
        for kind in range(2):
            for g in range(GROUPS):
                term = product(0, kind, g, cut)
                value = term if value is None else value + term
        out[:, columns(fs, k)] = value.astype(BF16)

    for df in range(1, n_fs):
        @pl.when(holder(fs_at(df)) == tp)
        def _(df=df):
            for c in range(X_CHUNKS):
                x_copy(df, c).wait_send()

        @pl.when(is_relay)
        def _(df=df):
            for c in range(X_CHUNKS):
                for dt in range(1, n_tp):
                    f_copy(df, c, dt).wait_send()

        for c in range(X_CHUNKS):
            first_copy(df, c).wait_send()
        for u in range(n_units):
            p_copy(df, u).wait_send()
    for dt in range(1, n_tp):
        @pl.when(own_holder)
        def _(dt=dt):
            own_copy(dt).wait_send()

        ss_copy(dt).wait_send()
        o_copy(dt).wait_send()
    for df, dt in h_order:
        for kind in range(2):
            for g in range(GROUPS):
                h_copy(df, dt, kind, g).wait_send()

    @pl.when(has_next)
    def _():
        for h in range(n_heads):
            st_copy(h).wait_send()

        def drain(slot, carry):
            for c in range(n_kv):
                kv_copy(slot, c).wait_send()
            return carry

        lax.fori_loop(0, sp + 1, drain, 0)

    for df in range(1, n_fs):
        for k in range(CHUNKS):
            m_copy(df, k).wait_recv()
            out[:, columns(fs_at(df), k)] = mrecv[df - 1, k]
    for df in range(1, n_fs):
        for k in range(CHUNKS):
            m_copy(df, k).wait_send()


def body(
    tokens, mix_gain, attn_query, attn_key, attn_value, rec_query, rec_forget, rec_input,
    break_offset, forget_room, out_gain, out_attn, out_rec,
):
    n_sp, n_fs, n_tp = lax.axis_size("sp"), lax.axis_size("fs"), lax.axis_size("tp")
    rows, feat_t = tokens.shape[1], tokens.shape[2]
    feat_f, cols = attn_query.shape
    width = feat_t * n_tp
    n_heads = cols // LANES
    out_rows, out_cols = out_attn.shape
    share = rows // n_tp
    piece = out_cols // CHUNKS
    n_sends = len(unit_list(cols)) + X_CHUNKS
    n_kv = X_CHUNKS + 2 * (GROUPS - 1)
    hbm = pl.BlockSpec(memory_space=pl.ANY)
    vmem = pl.BlockSpec(memory_space=pltpu.VMEM)
    dma = pltpu.SemaphoreType.DMA
    square = (n_heads, LANES, LANES)
    others = n_fs - 1
    result = pl.pallas_call(
        functools.partial(kernel, n_sp, n_fs, n_tp),
        out_shape=pltpu.VMEM((share, width), BF16),
        in_specs=[hbm] * 13,
        out_specs=vmem,
        scratch_shapes=[
            pltpu.VMEM((1, width), F32),
            pltpu.VMEM((1, n_heads), F32),
            pltpu.VMEM((n_heads, LANES), F32),
            pltpu.VMEM((1, LANES), F32),
            pltpu.VMEM((rows, feat_t), BF16),
            pltpu.VMEM((N_PROJ, feat_f, cols), BF16),
            pltpu.VMEM((n_tp, 2, out_rows, out_cols), BF16),
            pltpu.VMEM((n_fs, rows, feat_f), BF16),
            pltpu.VMEM((n_fs, rows, feat_f), BF16),
            pltpu.VMEM((n_tp, rows, LANES), F32),
            pltpu.VMEM((N_PROJ, rows, cols), F32),
            pltpu.VMEM((others, N_PROJ, rows, cols), BF16),
            pltpu.VMEM((others, N_PROJ, rows, cols), BF16),
            pltpu.VMEM((n_sp, 2 * GROUPS, rows, cols // GROUPS), BF16),
            pltpu.VMEM((rows, cols), BF16),
            pltpu.VMEM((rows, cols), BF16),
            pltpu.VMEM((rows, cols), F32),
            pltpu.VMEM((rows, cols), BF16),
            pltpu.VMEM((rows, cols), BF16),
            pltpu.VMEM((rows, cols), BF16),
            pltpu.VMEM((rows, cols), F32),
            pltpu.VMEM((n_heads, rows, LANES), F32),
            pltpu.VMEM((rows, cols), F32),
            pltpu.VMEM(square, F32),
            pltpu.VMEM((n_heads, 8, LANES), F32),
            pltpu.VMEM(square, BF16),
            pltpu.VMEM(square, BF16),
            pltpu.VMEM((2, rows, cols), BF16),
            pltpu.VMEM((n_fs, n_tp, 2, share, cols), BF16),
            pltpu.VMEM((others, share, out_cols), F32),
            pltpu.VMEM((others, CHUNKS, share, piece), BF16),
            pltpu.VMEM((others, CHUNKS, share, piece), BF16),
            dma((1,)), dma((N_SMALL,)), dma((N_PROJ + 2,)),
            dma((others * X_CHUNKS,)), dma((n_fs * X_CHUNKS,)), dma((others * X_CHUNKS * (n_tp - 1),)),
            dma((n_tp - 1,)), dma((1,)), dma((n_tp - 1,)), dma((n_tp,)),
            dma((others * n_sends,)), dma((others * n_sends,)),
            dma((n_sp * n_kv,)), dma((n_sp * n_kv,)),
            dma((n_heads,)), dma((n_heads,)),
            dma((n_tp - 1,)), dma((n_tp,)),
            dma((n_fs * n_tp * 2 * GROUPS,)), dma((n_fs * n_tp * 2 * GROUPS,)),
            dma((others * CHUNKS,)), dma((others * CHUNKS,)),
        ],
        compiler_params=pltpu.CompilerParams(
            collective_id=0, has_side_effects=True, vmem_limit_bytes=60 * 1024 * 1024
        ),
        name="layer",
    )(
        tokens.reshape(rows, feat_t), mix_gain.reshape(1, width),
        attn_key, attn_value, rec_forget, rec_input, attn_query, rec_query,
        break_offset.reshape(1, n_heads), forget_room, out_gain.reshape(1, LANES), out_attn, out_rec,
    )
    return result.reshape(1, share, width)


def solution(mesh):
    placed = (
        P(("grp", "fs"), "sp", "tp"),
        P(),
        P("fs", "tp"),
        P("fs", "tp"),
        P("fs", "tp"),
        P("fs", "tp"),
        P("fs", "tp"),
        P("fs", "tp"),
        P("tp"),
        P("tp", None),
        P(),
        P("tp", "fs"),
        P("tp", "fs"),
    )
    return jax.shard_map(
        body,
        mesh=mesh,
        in_specs=placed,
        out_specs=P(("grp", "fs"), ("sp", "tp"), None),
        check_vma=False,
    )
```

time: 44.8 us -> 41.7 us (0.931); the launches traced: 44.2 us -> 41.6 us
  Pallas kernels: 43.5 us -> 40.8 us
    pallas_call x1, Pallas kernels: 43.5 us -> 40.8 us  [body(): pl.pallas_call(functools.partial(kernel, n_sp, n_fs, n_tp), out_shape=plt...]
where the time goes in v2:
time: 41.7 us; the launch traced here: 41.6 us
  Pallas kernels  40.8 us (98%)
  local copies, waits for them, and re-layouts  0.71 us (2%)
    pallas_call x1, Pallas kernels, body(): pl.pallas_call(functools.partial(kernel, n_sp, n_fs, n_tp), out_shape=plt...  40.8 us

profile of v2, /device:TPU:26, one launch (start us, length us, event | category | flops | bytes accessed | tf_op | source)
XLA Modules:
  0.0 41.6 jit_solution(18292805439131924131)
XLA Ops:
  0.0 40.8 %layer.1 = bf16[64,2048]{1,0:T(8,128)(2,1)S(1)} custom-call(bf16[128,1024]{1,0:T(8,128)(2,1)} %bitcast.6, f32[1,2048]{1,0:T(1,128)} %bitcast.7, bf16[1024,512]{1,0:T(8,128)(2,1)} %w_k.1, bf16[1024,512]{1,0:T(8,128)(2,1)} %w_v.1, bf16[1024,512]{1,0:T(8,128)(2,1)} %w_f.1, bf16[1024,512]{1,0:T(8,128)(2,1)} %w_i.1, bf16[1024,512]{1,0:T(8,128)(2,1)} %w_q.1, ...), custom_call_target="tpu_custom_call" | custom-call | tf_op jit(solution)/shard_map/layer/pallas_call | solution.py:708
  40.8 0.7 %copy.15 = bf16[1,64,2048]{2,1,0:T(8,128)(2,1)} copy(bf16[1,64,2048]{2,1,0:T(8,128)(2,1)S(1)} %bitcast.5) | data formatting | bytes 524288

commit v3 on v2

--- a/solution.py
+++ b/solution.py
@@ -16,7 +16,7 @@
 N_PROJ = 6
 KEY, VALUE, FORGET, INPUT, QUERY, READ = range(N_PROJ)
 GROUPS = 2
-CHUNKS = 2
+CHUNKS = 4
 X_CHUNKS = 4
 N_SMALL = 4
 
@@ -40,10 +40,12 @@
 
 def unit_list(cols):
     g_cols = cols // GROUPS
-    units = [(w, 0) for w in (FORGET, INPUT)]
+    last = (GROUPS - 1) * g_cols
+    units = [(FORGET, 0), (INPUT, 0), (QUERY, last)]
     for g in range(1, GROUPS):
         units += [(w, g * g_cols) for w in (KEY, VALUE, FORGET, INPUT)]
-    units += [(w, g * g_cols) for w in (QUERY, READ) for g in range(GROUPS)]
+    units += [(QUERY, g * g_cols) for g in range(GROUPS - 1)]
+    units += [(READ, g * g_cols) for g in range(GROUPS)]
     return units
 
 
@@ -53,9 +55,9 @@
     out,
     gain, offs, room, out_gain,
     tok, wbuf, obuf, xt, xg, ss, acc, psend, precv, kv, qbuf, qdec, ecum, kinv, fresh, rec_i,
-    att, run, loc, st_loc, dec, st_in, st_out, heads, hrecv, part_acc, mix, mrecv,
+    att, run, q_back, v_back, v_far, loc, st_loc, dec, st_in, st_out, heads, hrecv, part_acc, mix, mrecv,
     t_sem, s_sem, w_sem, x_send, x_recv, f_send, own_send, own_recv, ss_send, ss_recv, p_send, p_recv,
-    kv_send, kv_recv, st_send, st_recv, o_send, o_recv, h_send, h_recv, m_send, m_recv,
+    kv_send, kv_recv, st_send, st_recv, o_send, o_recv, b_sem, h_send, h_recv, m_send, m_recv,
 ):
     sp, fs, tp = lax.axis_index("sp"), lax.axis_index("fs"), lax.axis_index("tp")
     rows, feat_t = tok.shape
@@ -73,6 +75,11 @@
     is_relay = tp == relay
     has_next = sp < n_sp - 1
     has_prev = sp > 0
+    back = n_sp > 3
+    at_end = sp == n_sp - 1
+    last = GROUPS - 1
+    near = sp < 3
+    far = sp >= 3
 
     def fs_at(step):
         return lax.rem(fs + step, n_fs)
@@ -108,12 +115,27 @@
         )
     ]
     w_copies = [
-        pltpu.make_async_copy(w, wbuf.at[i], w_sem.at[i])
+        pltpu.make_async_copy(w, wbuf.at[i], w_sem.at[i // 2])
         for i, w in enumerate((w_k, w_v, w_f, w_i, w_q, w_r))
     ]
     o_copies = [
-        pltpu.make_async_copy(w, obuf.at[tp, i], w_sem.at[N_PROJ + i]) for i, w in enumerate((o_attn, o_rec))
+        pltpu.make_async_copy(w, obuf.at[tp, i], w_sem.at[N_PROJ // 2]) for i, w in enumerate((o_attn, o_rec))
     ]
+
+    def w_wait(w):
+        pair = wbuf.at[pl.ds(w, 2)]
+        pltpu.make_async_copy(pair, pair, w_sem.at[w // 2]).wait()
+
+    def land(view, sem, wait_send=False):
+        copy = pltpu.make_async_remote_copy(
+            src_ref=view, dst_ref=view, send_sem=sem, recv_sem=sem,
+            device_id={"tp": tp_at(1)}, device_id_type=MESH,
+        )
+        if wait_send:
+            copy.wait_send()
+        else:
+            copy.wait_recv()
+
     for copy in small_copies + w_copies + o_copies:
         copy.start()
     tok_copy.wait()
@@ -134,7 +156,7 @@
     def x_copy(df, c):
         return pltpu.make_async_remote_copy(
             src_ref=tok.at[x_part(c), held(fs_at(df))], dst_ref=xt.at[fs, x_part(c)],
-            send_sem=x_send.at[(df - 1) * X_CHUNKS + c], recv_sem=x_recv.at[fs * X_CHUNKS + c],
+            send_sem=x_send.at[df - 1], recv_sem=x_recv.at[(n_fs - df - 1) * X_CHUNKS + c],
             device_id={"fs": fs_at(df), "tp": relay}, device_id_type=MESH,
         )
 
@@ -142,8 +164,8 @@
         slot = fs_at(df)
         return pltpu.make_async_remote_copy(
             src_ref=xt.at[slot, x_part(c)], dst_ref=xt.at[slot, x_part(c)],
-            send_sem=f_send.at[((df - 1) * X_CHUNKS + c) * (n_tp - 1) + dt - 1],
-            recv_sem=x_recv.at[slot * X_CHUNKS + c],
+            send_sem=f_send.at[(df - 1) * (n_tp - 1) + dt - 1],
+            recv_sem=x_recv.at[(df - 1) * X_CHUNKS + c],
             device_id={"tp": tp_at(dt)}, device_id_type=MESH,
         )
 
@@ -176,7 +198,7 @@
     def ss_copy(dt):
         return pltpu.make_async_remote_copy(
             src_ref=ss.at[tp], dst_ref=ss.at[tp],
-            send_sem=ss_send.at[dt - 1], recv_sem=ss_recv.at[tp],
+            send_sem=ss_send.at[dt - 1], recv_sem=ss_recv.at[n_tp - dt - 1],
             device_id={"tp": tp_at(dt)}, device_id_type=MESH,
         )
 
@@ -199,7 +221,7 @@
         return pltpu.make_async_remote_copy(
             src_ref=psend.at[df - 1, pl.ds(KEY, 2), x_part(c), pl.ds(0, g_cols)],
             dst_ref=precv.at[df - 1, pl.ds(KEY, 2), x_part(c), pl.ds(0, g_cols)],
-            send_sem=p_send.at[index], recv_sem=p_recv.at[index],
+            send_sem=p_send.at[df - 1], recv_sem=p_recv.at[index],
             device_id={"fs": fs_at(df)}, device_id_type=MESH,
         )
 
@@ -209,45 +231,33 @@
         return pltpu.make_async_remote_copy(
             src_ref=psend.at[df - 1, w, :, pl.ds(first, g_cols)],
             dst_ref=precv.at[df - 1, w, :, pl.ds(first, g_cols)],
-            send_sem=p_send.at[index], recv_sem=p_recv.at[index],
+            send_sem=p_send.at[df - 1], recv_sem=p_recv.at[index],
             device_id={"fs": fs_at(df)}, device_id_type=MESH,
         )
 
     @pl.when(jnp.logical_not(own_holder))
     def _():
-        pltpu.make_async_remote_copy(
-            src_ref=xt.at[fs], dst_ref=xt.at[fs], send_sem=own_send.at[0], recv_sem=own_recv.at[0],
-            device_id={"tp": tp_at(1)}, device_id_type=MESH,
-        ).wait_recv()
+        land(xt.at[fs], own_recv.at[0])
         xg[0] = (xt[fs].astype(F32) * gain_f).astype(BF16)
 
     total = ss[tp]
     for dt in range(1, n_tp):
         other = tp_at(dt)
-        pltpu.make_async_remote_copy(
-            src_ref=ss.at[other], dst_ref=ss.at[other],
-            send_sem=ss_send.at[dt - 1], recv_sem=ss_recv.at[other],
-            device_id={"tp": other}, device_id_type=MESH,
-        ).wait_recv()
+        land(ss.at[other], ss_recv.at[dt - 1])
         total = total + ss[other]
     factor = lax.rsqrt(jnp.sum(total, axis=1, keepdims=True) / width + norm_eps)
 
     def own_product(w, cut):
         acc[w, :, cut] = dot_nn(xg[0], wbuf[w, :, cut])
 
-    w_copies[KEY].wait()
+    w_wait(KEY)
     own_product(KEY, group(0))
-    w_copies[VALUE].wait()
     own_product(VALUE, group(0))
     for c in range(X_CHUNKS):
         part = slice(c * x_rows, (c + 1) * x_rows)
         for df in range(1, n_fs):
             slot = fs_at(df)
-            view = xt.at[slot, x_part(c)]
-            pltpu.make_async_remote_copy(
-                src_ref=view, dst_ref=view, send_sem=x_send.at[0], recv_sem=x_recv.at[slot * X_CHUNKS + c],
-                device_id={"tp": tp_at(1)}, device_id_type=MESH,
-            ).wait_recv()
+            land(xt.at[slot, x_part(c)], x_recv.at[(df - 1) * X_CHUNKS + c])
 
             @pl.when(is_relay)
             def _(df=df, c=c):
@@ -284,7 +294,7 @@
             view = kv.at[slot, 2 + c - X_CHUNKS]
         return pltpu.make_async_remote_copy(
             src_ref=view, dst_ref=view,
-            send_sem=kv_send.at[slot * n_kv + c], recv_sem=kv_recv.at[slot * n_kv + c],
+            send_sem=kv_send.at[slot], recv_sem=kv_recv.at[slot * n_kv + c],
             device_id={"sp": lax.rem(sp + 1, n_sp)}, device_id_type=MESH,
         )
 
@@ -315,8 +325,11 @@
 
     def hand_on(step, c):
         kv_copy(sp - step, c).wait_recv()
-
-        @pl.when(has_next)
+        goes_on = has_next
+        if back and c in group_kv(last):
+            goes_on = jnp.logical_and(has_next, jnp.logical_or(step < sp, sp < n_sp - 2))
+
+        @pl.when(goes_on)
         def _():
             kv_copy(sp - step, c).start()
 
@@ -324,26 +337,30 @@
         if step < n_sp:
             pl.when(sp >= step)(functools.partial(hand_on, step, c))
 
+    w_wait(FORGET)
+    quarter = X_CHUNKS // 4
     for w in (FORGET, INPUT):
-        w_copies[w].wait()
         partials(w, 0, cols)
         send_unit(w, 0)
-        finish_first(w - FORGET)
+        for c in range(quarter):
+            finish_first((w - FORGET) * quarter + c)
+    w_wait(QUERY)
+    partials(QUERY, 0, cols)
+    send_unit(QUERY, last)
     for w in (KEY, VALUE):
         partials(w, g_cols, cols - g_cols)
         for g in range(1, GROUPS):
             send_unit(w, g)
-        finish_first(2 + w)
-    for c in range(4, X_CHUNKS):
-        finish_first(c)
+        for c in range(quarter):
+            finish_first((2 + w) * quarter + c)
     for w in (FORGET, INPUT):
         for g in range(1, GROUPS):
             send_unit(w, g)
-    for w in (QUERY, READ):
-        w_copies[w].wait()
-        partials(w, 0, cols)
-        for g in range(GROUPS):
-            send_unit(w, g)
+    for g in range(last):
+        send_unit(QUERY, g)
+    partials(READ, 0, cols)
+    for g in range(GROUPS):
+        send_unit(READ, g)
     for w in (FORGET, INPUT):
         own_product(w, slice(0, cols))
     for w in (KEY, VALUE):
@@ -353,12 +370,11 @@
 
     def o_copy(dt):
         return pltpu.make_async_remote_copy(
-            src_ref=obuf.at[tp], dst_ref=obuf.at[tp], send_sem=o_send.at[dt - 1], recv_sem=o_recv.at[tp],
+            src_ref=obuf.at[tp], dst_ref=obuf.at[tp], send_sem=o_send.at[dt - 1], recv_sem=o_recv.at[n_tp - dt - 1],
             device_id={"tp": tp_at(dt)}, device_id_type=MESH,
         )
 
-    for copy in o_copies:
-        copy.wait()
+    pltpu.make_async_copy(obuf.at[tp], obuf.at[tp], w_sem.at[N_PROJ // 2]).wait()
     for dt in range(1, n_tp):
         o_copy(dt).start()
 
@@ -395,7 +411,7 @@
 
     def st_copy(h):
         return pltpu.make_async_remote_copy(
-            src_ref=st_out.at[h], dst_ref=st_in.at[h], send_sem=st_send.at[h], recv_sem=st_recv.at[h],
+            src_ref=st_out.at[h], dst_ref=st_in.at[h], send_sem=st_send.at[0], recv_sem=st_recv.at[h],
             device_id={"sp": lax.rem(sp + 1, n_sp)}, device_id_type=MESH,
         )
 
@@ -409,18 +425,21 @@
                 st_out[h] = st_loc[h].astype(BF16)
                 st_copy(h).start()
 
-    def state_step(g):
+    def state_step(h):
+        st_copy(h).wait_recv()
+
+        @pl.when(has_next)
+        def _():
+            st_out[h] = (st_in[h].astype(F32) * dec[h, 0:1, :] + st_loc[h]).astype(BF16)
+            st_copy(h).start()
+
+    def state_steps(g):
         for h in heads_of(g):
-            st_copy(h).wait_recv()
-
-            @pl.when(has_next)
-            def _(h=h):
-                st_out[h] = (st_in[h].astype(F32) * dec[h, 0:1, :] + st_loc[h]).astype(BF16)
-                st_copy(h).start()
+            state_step(h)
 
     def state_step_if(at, g):
         if at < n_sp:
-            pl.when(sp == at)(functools.partial(state_step, g))
+            pl.when(sp == at)(functools.partial(state_steps, g))
 
     def read_local(g):
         cut = group(g)
@@ -430,55 +449,57 @@
             scores = jnp.where(causal, dot_nt(qdec[:, lanes], kinv[:, lanes]), 0.0)
             loc[:, lanes] = dot_nn(scores.astype(BF16), rec_i[:, lanes])
 
-    n_parts = 2 * GROUPS
-
-    def h_copy(df, dt, kind, g):
-        index = ((df * n_tp + dt) * 2 + kind) * GROUPS + g
+    n_land = 2 + g_heads
+    early = pl.ds(0, last * g_cols)
+
+    def h_sem(df, dt, mark):
+        return h_recv.at[dt if df == 0 else n_tp + ((df - 1) * n_tp + dt) * n_land + mark]
+
+    def h_copy(df, dt, kind, first, count, mark):
         lands = (n_tp - dt) % n_tp
-        lands_index = ((df * n_tp + lands) * 2 + kind) * GROUPS + g
-        return pltpu.make_async_remote_copy(
-            src_ref=heads.at[kind, pl.ds(pl.multiple_of(tp_at(dt) * share, share), share), pl.ds(g * g_cols, g_cols)],
-            dst_ref=hrecv.at[df, lands, kind, :, pl.ds(g * g_cols, g_cols)],
-            send_sem=h_send.at[index], recv_sem=h_recv.at[lands_index],
+        lanes = pl.ds(first, count)
+        return pltpu.make_async_remote_copy(
+            src_ref=heads.at[kind, pl.ds(pl.multiple_of(tp_at(dt) * share, share), share), lanes],
+            dst_ref=hrecv.at[df, lands, kind, :, lanes],
+            send_sem=h_send.at[df * n_tp + dt], recv_sem=h_sem(df, lands, mark),
             device_id={"fs": fs_at(df), "tp": tp_at(dt)}, device_id_type=MESH,
         )
 
     h_order = [(df, dt) for df in list(range(1, n_fs)) + [0] for dt in range(n_tp) if df or dt]
 
-    def h_wait(df, dt, kind, g):
-        view = hrecv.at[df, dt, kind, :, pl.ds(g * g_cols, g_cols)]
-        pltpu.make_async_remote_copy(
-            src_ref=view, dst_ref=view, send_sem=h_send.at[0],
-            recv_sem=h_recv.at[((df * n_tp + dt) * 2 + kind) * GROUPS + g],
-            device_id={"tp": tp_at(1)}, device_id_type=MESH,
-        ).wait_recv()
+    def send_heads(kind, first, count, mark):
+        for df, dt in h_order:
+            h_copy(df, dt, kind, first, count, mark).start()
 
     def send_attn(g):
         heads[0, :, group(g)] = att[:, group(g)].astype(BF16)
-        for df, dt in h_order:
-            h_copy(df, dt, 0, g).start()
-
-    def send_attn_if(condition, g):
-        pl.when(condition)(functools.partial(send_attn, g))
+        send_heads(0, g * g_cols, g_cols, 1 if g == last else 0)
+
+    def finish_rec(h):
+        lanes = lanes_of(h)
+
+        @pl.when(has_prev)
+        def _():
+            loc[:, lanes] += dot_nt(qdec[:, lanes], st_in[h])
+
+        raw = loc[:, lanes]
+        norm = lax.rsqrt(jnp.mean(raw * raw, axis=1, keepdims=True) + norm_eps)
+        heads[1, :, lanes] = (raw * norm * out_gain[...]).astype(BF16)
 
     def send_rec(g):
-        for h in heads_of(g):
-            lanes = lanes_of(h)
-
-            @pl.when(has_prev)
-            def _(h=h, lanes=lanes):
-                loc[:, lanes] += dot_nt(qdec[:, lanes], st_in[h])
-
-            raw = loc[:, lanes]
-            norm = lax.rsqrt(jnp.mean(raw * raw, axis=1, keepdims=True) + norm_eps)
-            heads[1, :, lanes] = (raw * norm * out_gain[...]).astype(BF16)
-        for df, dt in h_order:
-            h_copy(df, dt, 1, g).start()
-
-    def attend(slot, g, diagonal):
+        for i, h in enumerate(heads_of(g)):
+            if g == last:
+                pl.when(far)(functools.partial(state_step, h))
+            finish_rec(h)
+            if g == last:
+                send_heads(1, h * LANES, LANES, 2 + i)
+        if g < last:
+            send_heads(1, g * g_cols, g_cols, 0)
+
+    def sticks(queries, slot, g, diagonal):
         z = jnp.concatenate(
             [
-                dot_nt(qbuf[:, lanes_of(h)], kv[slot, 2 * g, :, lanes_of(i)]) * scale + offs[0:1, h:h + 1]
+                dot_nt(queries[:, lanes_of(i)], kv[slot, 2 * g, :, lanes_of(i)]) * scale + offs[0:1, h:h + 1]
                 for i, h in enumerate(heads_of(g))
             ],
             axis=0,
@@ -491,7 +512,10 @@
         stick = jnp.exp(log_stick + both[:, :rows])
         if diagonal:
             stick = jnp.where(strict, stick, 0.0)
-        stick = stick.astype(BF16)
+        return stick.astype(BF16), both
+
+    def attend(slot, g, diagonal):
+        stick, both = sticks(qbuf.at[:, group(g)], slot, g, diagonal)
         for i, h in enumerate(heads_of(g)):
             mine = slice(i * rows, (i + 1) * rows)
             value = dot_nn(stick[mine], kv[slot, 2 * g + 1, :, lanes_of(i)])
@@ -514,16 +538,48 @@
             attend(sp - step, g, False)
             return carry
 
-        lax.fori_loop(3, sp + 1, block, 0)
-
-    near = sp < 3
-    far = sp >= 3
+        end = sp + 1
+        if back and g == last:
+            end = jnp.where(at_end, sp, sp + 1)
+        lax.fori_loop(3, end, block, 0)
+
+    def q_copy():
+        return pltpu.make_async_remote_copy(
+            src_ref=qbuf.at[:, pl.ds(last * g_cols, g_cols)], dst_ref=q_back,
+            send_sem=b_sem.at[0], recv_sem=b_sem.at[0], device_id={"sp": 0}, device_id_type=MESH,
+        )
+
+    def v_copy():
+        return pltpu.make_async_remote_copy(
+            src_ref=v_back, dst_ref=v_far,
+            send_sem=b_sem.at[1], recv_sem=b_sem.at[1], device_id={"sp": n_sp - 1}, device_id_type=MESH,
+        )
+
+    def ask_back():
+        q_copy().start()
+
+    def answer():
+        q_copy().wait_recv()
+        stick, _ = sticks(q_back, 0, last, False)
+        for i in range(g_heads):
+            value = dot_nn(stick[i * rows:(i + 1) * rows], kv[0, 2 * last + 1, :, lanes_of(i)])
+            v_back[:, lanes_of(i)] = value.astype(BF16)
+        v_copy().start()
+
+    def take_answer():
+        v_copy().wait_recv()
+        for i, h in enumerate(heads_of(last)):
+            att[:, lanes_of(h)] += v_far[:, lanes_of(i)].astype(F32) * jnp.exp(run[h])
+
     for c in group_kv(0):
         hand_on_if(1, c)
     gates(0)
     local_state(0)
+    qbuf[:, group(last)] = finish(QUERY, last)
     for c in group_kv(0):
         hand_on_if(2, c)
+        if back and c == 0:
+            pl.when(at_end)(ask_back)
     for g in range(1, GROUPS):
         for w in (KEY, VALUE):
             finish_kv(w, g)
@@ -534,53 +590,57 @@
         local_state(g)
         hand_on_if(1, group_kv(g)[1])
     state_step_if(2, 0)
-    qbuf[:, group(0)] = finish(QUERY, 0)
-    attend(sp, 0, True)
-    attend_if(1, 0)
-    attend_if(2, 0)
-    attend_rest(0)
-    send_attn(0)
+    for g in range(last):
+        qbuf[:, group(g)] = finish(QUERY, g)
+        attend(sp, g, True)
+        attend_if(1, g)
+        attend_if(2, g)
+        attend_rest(g)
+        send_attn(g)
+    for g in range(1, GROUPS):
+        state_step_if(1, g)
+        attend(sp, g, True)
+        attend_if(1, g)
+
+        @pl.when(sp < 2)
+        def _(g=g):
+            send_attn(g)
+
+    if back:
+        pl.when(sp == 0)(answer)
+    read_local(0)
+
+    @pl.when(near)
+    def _():
+        send_rec(0)
+
     for g in range(1, GROUPS):
         hand_on_if(2, group_kv(g)[0])
-        state_step_if(1, g)
-        qbuf[:, group(g)] = finish(QUERY, g)
-        attend(sp, g, True)
+        read_local(g)
+        state_step_if(2, g)
         hand_on_if(2, group_kv(g)[1])
-    read_local(0)
-
-    @pl.when(far)
-    def _():
-        state_step(0)
-
-    send_rec(0)
-    for g in range(1, GROUPS):
-        attend_if(1, g)
-        state_step_if(2, g)
         attend_if(2, g)
-
-        @pl.when(near)
-        def _(g=g):
-            send_attn(g)
-
-        read_local(g)
-
-        @pl.when(near)
-        def _(g=g):
-            send_rec(g)
 
         @pl.when(far)
         def _(g=g):
             attend_rest(g)
+            if back and g == last:
+                pl.when(at_end)(take_answer)
+
+        @pl.when(sp >= 2)
+        def _(g=g):
             send_attn(g)
-            state_step(g)
-            send_rec(g)
+
+        @pl.when(far)
+        def _(g=g):
+            state_steps(g - 1)
+            send_rec(g - 1)
+
+        send_rec(g)
 
     for dt in range(1, n_tp):
         other = tp_at(dt)
-        pltpu.make_async_remote_copy(
-            src_ref=obuf.at[other], dst_ref=obuf.at[other], send_sem=o_send.at[dt - 1], recv_sem=o_recv.at[other],
-            device_id={"tp": other}, device_id_type=MESH,
-        ).wait_recv()
+        land(obuf.at[other], o_recv.at[dt - 1])
 
     half = out_cols // CHUNKS
 
@@ -588,71 +648,63 @@
         index = (df - 1) * CHUNKS + k
         return pltpu.make_async_remote_copy(
             src_ref=mix.at[df - 1, k], dst_ref=mrecv.at[df - 1, k],
-            send_sem=m_send.at[index], recv_sem=m_recv.at[index],
+            send_sem=m_send.at[df - 1], recv_sem=m_recv.at[index],
             device_id={"fs": fs_at(n_fs - df)}, device_id_type=MESH,
         )
 
     def columns(owner, k):
         return pl.ds(pl.multiple_of(owner * out_cols + k * half, LANES), half)
 
-    def product(df, kind, g, cut):
+    def product(df, kind, lanes, cut):
         value = None
         for dt in range(n_tp):
             if df == 0 and dt == 0:
-                left = heads[kind, pl.ds(pl.multiple_of(tp * share, share), share), group(g)]
+                left = heads[kind, pl.ds(pl.multiple_of(tp * share, share), share), lanes]
             else:
-                left = hrecv[df, dt, kind, :, group(g)]
-            term = dot_nn(left, obuf[tp_at(dt), kind, group(g), cut])
+                left = hrecv[df, dt, kind, :, lanes]
+            term = dot_nn(left, obuf[tp_at(dt), kind, lanes, cut])
             value = term if value is None else value + term
         return value
 
     whole = slice(0, out_cols)
-    pieces = [(kind, g) for g in range(GROUPS) for kind in range(2)]
+    final = lanes_of(n_heads - 1)
     for df in range(1, n_fs):
-        for place, (kind, g) in enumerate(pieces[:-1]):
+        for dt in range(n_tp):
+            land(hrecv.at[df, dt, :, :, early], h_sem(df, dt, 0))
+        for kind in range(2):
+            for g in range(last):
+                if kind == 0 and g == 0:
+                    part_acc[df - 1] = product(df, kind, group(g), whole)
+                else:
+                    part_acc[df - 1] += product(df, kind, group(g), whole)
+        marks = [(0, group(last))] + [(1, lanes_of(h)) for h in heads_of(last)]
+        for mark, (kind, lanes) in enumerate(marks):
             for dt in range(n_tp):
-                h_wait(df, dt, kind, g)
-            if place == 0:
-                part_acc[df - 1] = product(df, kind, g, whole)
-            else:
-                part_acc[df - 1] += product(df, kind, g, whole)
-    for df in range(1, n_fs):
-        kind, g = pieces[-1]
-        for dt in range(n_tp):
-            h_wait(df, dt, kind, g)
+                land(hrecv.at[df, dt, kind, :, lanes], h_sem(df, dt, 1 + mark))
+            if mark < len(marks) - 1:
+                part_acc[df - 1] += product(df, kind, lanes, whole)
         for k in range(CHUNKS):
             cut = slice(k * half, (k + 1) * half)
-            mix[df - 1, k] = (part_acc[df - 1, :, cut] + product(df, kind, g, cut)).astype(BF16)
+            mix[df - 1, k] = (part_acc[df - 1, :, cut] + product(df, 1, final, cut)).astype(BF16)
             m_copy(df, k).start()
     for dt in range(1, n_tp):
-        for kind in range(2):
-            for g in range(GROUPS):
-                h_wait(0, dt, kind, g)
+        land(hrecv.at[0, dt], h_sem(0, dt, 0))
     for k in range(CHUNKS):
         cut = slice(k * half, (k + 1) * half)
-        value = None
-        for kind in range(2):
-            for g in range(GROUPS):
-                term = product(0, kind, g, cut)
-                value = term if value is None else value + term
+        value = product(0, 0, slice(0, cols), cut) + product(0, 1, slice(0, cols), cut)
         out[:, columns(fs, k)] = value.astype(BF16)
 
     for df in range(1, n_fs):
         @pl.when(holder(fs_at(df)) == tp)
         def _(df=df):
-            for c in range(X_CHUNKS):
-                x_copy(df, c).wait_send()
+            land(xt.at[0], x_send.at[df - 1], True)
 
         @pl.when(is_relay)
         def _(df=df):
-            for c in range(X_CHUNKS):
-                for dt in range(1, n_tp):
-                    f_copy(df, c, dt).wait_send()
-
-        for c in range(X_CHUNKS):
-            first_copy(df, c).wait_send()
-        for u in range(n_units):
-            p_copy(df, u).wait_send()
+            for dt in range(1, n_tp):
+                land(xt.at[0], f_send.at[(df - 1) * (n_tp - 1) + dt - 1], True)
+
+        land(psend.at[df - 1], p_send.at[df - 1], True)
     for dt in range(1, n_tp):
         @pl.when(own_holder)
         def _(dt=dt):
@@ -661,29 +713,42 @@
         ss_copy(dt).wait_send()
         o_copy(dt).wait_send()
     for df, dt in h_order:
-        for kind in range(2):
-            for g in range(GROUPS):
-                h_copy(df, dt, kind, g).wait_send()
+        land(hrecv.at[df, dt], h_send.at[df * n_tp + dt], True)
 
     @pl.when(has_next)
     def _():
-        for h in range(n_heads):
-            st_copy(h).wait_send()
+        land(st_out, st_send.at[0], True)
 
         def drain(slot, carry):
-            for c in range(n_kv):
-                kv_copy(slot, c).wait_send()
+            land(kv.at[slot], kv_send.at[slot], True)
             return carry
 
-        lax.fori_loop(0, sp + 1, drain, 0)
+        if back:
+            shorter = sp == n_sp - 2
+
+            @pl.when(shorter)
+            def _():
+                land(kv.at[0, pl.ds(0, 2 * last)], kv_send.at[0], True)
+
+            lax.fori_loop(jnp.where(shorter, 1, 0), sp + 1, drain, 0)
+        else:
+            lax.fori_loop(0, sp + 1, drain, 0)
+
+    if back:
+        @pl.when(at_end)
+        def _():
+            q_copy().wait_send()
+
+        @pl.when(sp == 0)
+        def _():
+            v_copy().wait_send()
 
     for df in range(1, n_fs):
         for k in range(CHUNKS):
             m_copy(df, k).wait_recv()
             out[:, columns(fs_at(df), k)] = mrecv[df - 1, k]
     for df in range(1, n_fs):
-        for k in range(CHUNKS):
-            m_copy(df, k).wait_send()
+        land(mix.at[df - 1], m_send.at[df - 1], True)
 
 
 def body(
@@ -733,6 +798,9 @@
             pltpu.VMEM((rows, cols), BF16),
             pltpu.VMEM((rows, cols), F32),
             pltpu.VMEM((n_heads, rows, LANES), F32),
+            pltpu.VMEM((rows, cols // GROUPS), BF16),
+            pltpu.VMEM((rows, cols // GROUPS), BF16),
+            pltpu.VMEM((rows, cols // GROUPS), BF16),
             pltpu.VMEM((rows, cols), F32),
             pltpu.VMEM(square, F32),
             pltpu.VMEM((n_heads, 8, LANES), F32),
@@ -743,15 +811,15 @@
             pltpu.VMEM((others, share, out_cols), F32),
             pltpu.VMEM((others, CHUNKS, share, piece), BF16),
             pltpu.VMEM((others, CHUNKS, share, piece), BF16),
-            dma((1,)), dma((N_SMALL,)), dma((N_PROJ + 2,)),
-            dma((others * X_CHUNKS,)), dma((n_fs * X_CHUNKS,)), dma((others * X_CHUNKS * (n_tp - 1),)),
-            dma((n_tp - 1,)), dma((1,)), dma((n_tp - 1,)), dma((n_tp,)),
-            dma((others * n_sends,)), dma((others * n_sends,)),
-            dma((n_sp * n_kv,)), dma((n_sp * n_kv,)),
-            dma((n_heads,)), dma((n_heads,)),
-            dma((n_tp - 1,)), dma((n_tp,)),
-            dma((n_fs * n_tp * 2 * GROUPS,)), dma((n_fs * n_tp * 2 * GROUPS,)),
-            dma((others * CHUNKS,)), dma((others * CHUNKS,)),
+            dma((1,)), dma((N_SMALL,)), dma((N_PROJ // 2 + 1,)),
+            dma((others,)), dma((others * X_CHUNKS,)), dma((others * (n_tp - 1),)),
+            dma((n_tp - 1,)), dma((1,)), dma((n_tp - 1,)), dma((n_tp - 1,)),
+            dma((others,)), dma((others * n_sends,)),
+            dma((n_sp,)), dma(((n_sp - 1) * n_kv,)),
+            dma((1,)), dma((n_heads,)),
+            dma((n_tp - 1,)), dma((n_tp - 1,)), dma((2,)),
+            dma((n_fs * n_tp,)), dma((n_tp + others * n_tp * (2 + n_heads // GROUPS),)),
+            dma((others,)), dma((others * CHUNKS,)),
         ],
         compiler_params=pltpu.CompilerParams(
             collective_id=0, has_side_effects=True, vmem_limit_bytes=60 * 1024 * 1024

time: 41.7 us -> 39.6 us (0.950)
  Pallas kernels: 40.8 us -> 38.8 us
    pallas_call x1, Pallas kernels: 40.8 us -> 38.8 us  [body(): pl.pallas_call(functools.partial(kernel, n_sp, n_fs, n_tp), out_shape=plt...]
where the time goes in v3:
time: 39.6 us; the launch traced here: 39.5 us
  Pallas kernels  38.8 us (98%)
  local copies, waits for them, and re-layouts  0.71 us (2%)
    pallas_call x1, Pallas kernels, body(): pl.pallas_call(functools.partial(kernel, n_sp, n_fs, n_tp), out_shape=plt...  38.8 us

profile of v3, /device:TPU:26, one launch (start us, length us, event | category | flops | bytes accessed | tf_op | source)
XLA Modules:
  0.0 39.5 jit_solution(11648365792565731012)
XLA Ops:
  0.0 38.8 %layer.1 = bf16[64,2048]{1,0:T(8,128)(2,1)S(1)} custom-call(bf16[128,1024]{1,0:T(8,128)(2,1)} %bitcast.6, f32[1,2048]{1,0:T(1,128)} %bitcast.7, bf16[1024,512]{1,0:T(8,128)(2,1)} %w_k.1, bf16[1024,512]{1,0:T(8,128)(2,1)} %w_v.1, bf16[1024,512]{1,0:T(8,128)(2,1)} %w_f.1, bf16[1024,512]{1,0:T(8,128)(2,1)} %w_i.1, bf16[1024,512]{1,0:T(8,128)(2,1)} %w_q.1, ...), custom_call_target="tpu_custom_call" | custom-call | tf_op jit(solution)/shard_map/layer/pallas_call | solution.py:773
  38.8 0.7 %copy.15 = bf16[1,64,2048]{2,1,0:T(8,128)(2,1)} copy(bf16[1,64,2048]{2,1,0:T(8,128)(2,1)S(1)} %bitcast.5) | data formatting | bytes 524288

commit v4 on v3

--- a/solution.py
+++ b/solution.py
@@ -19,6 +19,7 @@
 CHUNKS = 4
 X_CHUNKS = 4
 N_SMALL = 4
+N_ASK = 2
 
 
 def dot_nn(a, b):
@@ -55,9 +56,9 @@
     out,
     gain, offs, room, out_gain,
     tok, wbuf, obuf, xt, xg, ss, acc, psend, precv, kv, qbuf, qdec, ecum, kinv, fresh, rec_i,
-    att, run, q_back, v_back, v_far, loc, st_loc, dec, st_in, st_out, heads, hrecv, part_acc, mix, mrecv,
+    att, run, q_back, v_back, v_far, loc, st_loc, dec, st_in, st_out, heads, hrecv, part_acc, mix,
     t_sem, s_sem, w_sem, x_send, x_recv, f_send, own_send, own_recv, ss_send, ss_recv, p_send, p_recv,
-    kv_send, kv_recv, st_send, st_recv, o_send, o_recv, b_sem, h_send, h_recv, m_send, m_recv,
+    kv_send, kv_recv, st_send, st_recv, o_send, o_recv, b_sem, h_send, h_recv, m_send, m_recv, ready,
 ):
     sp, fs, tp = lax.axis_index("sp"), lax.axis_index("fs"), lax.axis_index("tp")
     rows, feat_t = tok.shape
@@ -75,8 +76,9 @@
     is_relay = tp == relay
     has_next = sp < n_sp - 1
     has_prev = sp > 0
-    back = n_sp > 3
-    at_end = sp == n_sp - 1
+    n_ask = min(N_ASK, n_sp - 2)
+    first_ask = n_sp - n_ask
+    asks = sp >= first_ask
     last = GROUPS - 1
     near = sp < 3
     far = sp >= 3
@@ -104,9 +106,6 @@
     def _():
         pl.semaphore_signal(barrier, inc=1, device_id={"sp": sp + 1}, device_id_type=MESH)
 
-    @pl.when(has_prev)
-    def _():
-        pl.semaphore_signal(barrier, inc=1, device_id={"sp": sp - 1}, device_id_type=MESH)
 
     small_copies = [
         pltpu.make_async_copy(source, target, s_sem.at[i])
@@ -140,9 +139,11 @@
         copy.start()
     tok_copy.wait()
 
-    next_count = jnp.where(has_next, 1, 0)
-    prev_count = jnp.where(has_prev, 1, 0)
-    pl.semaphore_wait(barrier, n_fs * n_tp - 1 + next_count + prev_count)
+    pl.semaphore_wait(barrier, n_fs * n_tp - 1 + jnp.where(has_prev, 1, 0))
+
+    @pl.when(has_prev)
+    def _():
+        pl.semaphore_signal(ready, inc=1, device_id={"sp": sp - 1}, device_id_type=MESH)
 
     def holder(f_index):
         return (f_index * feat_f) // feat_t
@@ -326,16 +327,24 @@
     def hand_on(step, c):
         kv_copy(sp - step, c).wait_recv()
         goes_on = has_next
-        if back and c in group_kv(last):
-            goes_on = jnp.logical_and(has_next, jnp.logical_or(step < sp, sp < n_sp - 2))
+        if c in group_kv(last):
+            goes_on = jnp.logical_and(has_next, jnp.logical_or(step < sp, sp + 1 < first_ask))
 
         @pl.when(goes_on)
         def _():
             kv_copy(sp - step, c).start()
 
+    def from_step(step, g):
+        return step + 1 if g == last and step >= first_ask else step
+
     def hand_on_if(step, c):
         if step < n_sp:
-            pl.when(sp >= step)(functools.partial(hand_on, step, c))
+            g = last if c in group_kv(last) else 0
+            pl.when(sp >= from_step(step, g))(functools.partial(hand_on, step, c))
+
+    @pl.when(has_next)
+    def _():
+        pl.semaphore_wait(ready, 1)
 
     w_wait(FORGET)
     quarter = X_CHUNKS // 4
@@ -346,7 +355,7 @@
             finish_first((w - FORGET) * quarter + c)
     w_wait(QUERY)
     partials(QUERY, 0, cols)
-    send_unit(QUERY, last)
+    pl.when(has_prev)(functools.partial(send_unit, QUERY, last))
     for w in (KEY, VALUE):
         partials(w, g_cols, cols - g_cols)
         for g in range(1, GROUPS):
@@ -356,6 +365,7 @@
     for w in (FORGET, INPUT):
         for g in range(1, GROUPS):
             send_unit(w, g)
+    pl.when(sp == 0)(functools.partial(send_unit, QUERY, last))
     for g in range(last):
         send_unit(QUERY, g)
     partials(READ, 0, cols)
@@ -433,13 +443,16 @@
             st_out[h] = (st_in[h].astype(F32) * dec[h, 0:1, :] + st_loc[h]).astype(BF16)
             st_copy(h).start()
 
-    def state_steps(g):
-        for h in heads_of(g):
+    def state_steps(g, half=None):
+        mine = heads_of(g)
+        if half is not None:
+            mine = mine[:1] if half == 0 else mine[1:]
+        for h in mine:
             state_step(h)
 
-    def state_step_if(at, g):
+    def state_step_if(at, g, half=None):
         if at < n_sp:
-            pl.when(sp == at)(functools.partial(state_steps, g))
+            pl.when(sp == at)(functools.partial(state_steps, g, half))
 
     def read_local(g):
         cut = group(g)
@@ -529,7 +542,7 @@
 
     def attend_if(step, g):
         if step < n_sp:
-            pl.when(sp >= step)(functools.partial(attend, sp - step, g, False))
+            pl.when(sp >= from_step(step, g))(functools.partial(attend, sp - step, g, False))
 
     def attend_rest(g):
         def block(step, carry):
@@ -538,36 +551,43 @@
             attend(sp - step, g, False)
             return carry
 
-        end = sp + 1
-        if back and g == last:
-            end = jnp.where(at_end, sp, sp + 1)
+        end = jnp.where(asks, sp, sp + 1) if g == last else sp + 1
         lax.fori_loop(3, end, block, 0)
 
-    def q_copy():
-        return pltpu.make_async_remote_copy(
-            src_ref=qbuf.at[:, pl.ds(last * g_cols, g_cols)], dst_ref=q_back,
-            send_sem=b_sem.at[0], recv_sem=b_sem.at[0], device_id={"sp": 0}, device_id_type=MESH,
-        )
-
-    def v_copy():
-        return pltpu.make_async_remote_copy(
-            src_ref=v_back, dst_ref=v_far,
-            send_sem=b_sem.at[1], recv_sem=b_sem.at[1], device_id={"sp": n_sp - 1}, device_id_type=MESH,
+    def q_copy(asker):
+        return pltpu.make_async_remote_copy(
+            src_ref=qbuf.at[:, pl.ds(last * g_cols, g_cols)], dst_ref=q_back.at[asker],
+            send_sem=b_sem.at[asker], recv_sem=b_sem.at[asker], device_id={"sp": 0}, device_id_type=MESH,
+        )
+
+    def v_copy(asker):
+        return pltpu.make_async_remote_copy(
+            src_ref=v_back.at[asker], dst_ref=v_far,
+            send_sem=b_sem.at[n_ask + asker], recv_sem=b_sem.at[n_ask + asker],
+            device_id={"sp": first_ask + asker}, device_id_type=MESH,
         )
 
     def ask_back():
-        q_copy().start()
+        for asker in range(n_ask):
+            @pl.when(sp == first_ask + asker)
+            def _(asker=asker):
+                q_copy(asker).start()
 
     def answer():
-        q_copy().wait_recv()
-        stick, _ = sticks(q_back, 0, last, False)
-        for i in range(g_heads):
-            value = dot_nn(stick[i * rows:(i + 1) * rows], kv[0, 2 * last + 1, :, lanes_of(i)])
-            v_back[:, lanes_of(i)] = value.astype(BF16)
-        v_copy().start()
+        for asker in reversed(range(n_ask)):
+            q_copy(asker).wait_recv()
+            stick, _ = sticks(q_back.at[asker], 0, last, False)
+            for i in range(g_heads):
+                value = dot_nn(stick[i * rows:(i + 1) * rows], kv[0, 2 * last + 1, :, lanes_of(i)])
+                v_back[asker, :, lanes_of(i)] = value.astype(BF16)
+            v_copy(asker).start()
 
     def take_answer():
-        v_copy().wait_recv()
+        for asker in range(n_ask):
+            @pl.when(sp == first_ask + asker)
+            def _(asker=asker):
+                v_copy(asker).wait_recv()
+
         for i, h in enumerate(heads_of(last)):
             att[:, lanes_of(h)] += v_far[:, lanes_of(i)].astype(F32) * jnp.exp(run[h])
 
@@ -575,11 +595,15 @@
         hand_on_if(1, c)
     gates(0)
     local_state(0)
-    qbuf[:, group(last)] = finish(QUERY, last)
+
+    def last_queries():
+        qbuf[:, group(last)] = finish(QUERY, last)
+
+    pl.when(has_prev)(last_queries)
     for c in group_kv(0):
         hand_on_if(2, c)
-        if back and c == 0:
-            pl.when(at_end)(ask_back)
+        if c == 0 and n_sp <= 4:
+            ask_back()
     for g in range(1, GROUPS):
         for w in (KEY, VALUE):
             finish_kv(w, g)
@@ -590,6 +614,9 @@
         local_state(g)
         hand_on_if(1, group_kv(g)[1])
     state_step_if(2, 0)
+    pl.when(sp == 0)(last_queries)
+    for g in range(1, GROUPS):
+        state_step_if(1, g)
     for g in range(last):
         qbuf[:, group(g)] = finish(QUERY, g)
         attend(sp, g, True)
@@ -597,8 +624,11 @@
         attend_if(2, g)
         attend_rest(g)
         send_attn(g)
+    if n_sp > 4:
+        ask_back()
+    if n_ask:
+        pl.when(sp == 0)(answer)
     for g in range(1, GROUPS):
-        state_step_if(1, g)
         attend(sp, g, True)
         attend_if(1, g)
 
@@ -606,8 +636,7 @@
         def _(g=g):
             send_attn(g)
 
-    if back:
-        pl.when(sp == 0)(answer)
+    state_step_if(2, last, 0)
     read_local(0)
 
     @pl.when(near)
@@ -615,17 +644,19 @@
         send_rec(0)
 
     for g in range(1, GROUPS):
+        read_local(g)
+        if g == last:
+            state_step_if(2, g, 1)
         hand_on_if(2, group_kv(g)[0])
-        read_local(g)
-        state_step_if(2, g)
         hand_on_if(2, group_kv(g)[1])
         attend_if(2, g)
 
         @pl.when(far)
         def _(g=g):
             attend_rest(g)
-            if back and g == last:
-                pl.when(at_end)(take_answer)
+
+        if g == last:
+            pl.when(asks)(take_answer)
 
         @pl.when(sp >= 2)
         def _(g=g):
@@ -644,16 +675,15 @@
 
     half = out_cols // CHUNKS
 
-    def m_copy(df, k):
-        index = (df - 1) * CHUNKS + k
-        return pltpu.make_async_remote_copy(
-            src_ref=mix.at[df - 1, k], dst_ref=mrecv.at[df - 1, k],
-            send_sem=m_send.at[df - 1], recv_sem=m_recv.at[index],
-            device_id={"fs": fs_at(n_fs - df)}, device_id_type=MESH,
-        )
-
     def columns(owner, k):
         return pl.ds(pl.multiple_of(owner * out_cols + k * half, LANES), half)
+
+    def m_copy(df, k):
+        return pltpu.make_async_remote_copy(
+            src_ref=mix.at[df - 1, k], dst_ref=out.at[:, columns(fs, k)],
+            send_sem=m_send.at[df - 1], recv_sem=m_recv.at[df - 1],
+            device_id={"fs": fs_at(n_fs - df)}, device_id_type=MESH,
+        )
 
     def product(df, kind, lanes, cut):
         value = None
@@ -723,31 +753,25 @@
             land(kv.at[slot], kv_send.at[slot], True)
             return carry
 
-        if back:
-            shorter = sp == n_sp - 2
-
-            @pl.when(shorter)
-            def _():
-                land(kv.at[0, pl.ds(0, 2 * last)], kv_send.at[0], True)
-
-            lax.fori_loop(jnp.where(shorter, 1, 0), sp + 1, drain, 0)
-        else:
-            lax.fori_loop(0, sp + 1, drain, 0)
-
-    if back:
-        @pl.when(at_end)
+        shorter = sp + 1 >= first_ask
+
+        @pl.when(shorter)
         def _():
-            q_copy().wait_send()
+            land(kv.at[0, pl.ds(0, 2 * last)], kv_send.at[0], True)
+
+        lax.fori_loop(jnp.where(shorter, 1, 0), sp + 1, drain, 0)
+
+    for asker in range(n_ask):
+        @pl.when(sp == first_ask + asker)
+        def _(asker=asker):
+            q_copy(asker).wait_send()
 
         @pl.when(sp == 0)
-        def _():
-            v_copy().wait_send()
+        def _(asker=asker):
+            v_copy(asker).wait_send()
 
     for df in range(1, n_fs):
-        for k in range(CHUNKS):
-            m_copy(df, k).wait_recv()
-            out[:, columns(fs_at(df), k)] = mrecv[df - 1, k]
-    for df in range(1, n_fs):
+        land(mix.at[df - 1], m_recv.at[df - 1])
         land(mix.at[df - 1], m_send.at[df - 1], True)
 
 
@@ -765,6 +789,7 @@
     piece = out_cols // CHUNKS
     n_sends = len(unit_list(cols)) + X_CHUNKS
     n_kv = X_CHUNKS + 2 * (GROUPS - 1)
+    n_ask = min(N_ASK, n_sp - 2)
     hbm = pl.BlockSpec(memory_space=pl.ANY)
     vmem = pl.BlockSpec(memory_space=pltpu.VMEM)
     dma = pltpu.SemaphoreType.DMA
@@ -798,8 +823,8 @@
             pltpu.VMEM((rows, cols), BF16),
             pltpu.VMEM((rows, cols), F32),
             pltpu.VMEM((n_heads, rows, LANES), F32),
-            pltpu.VMEM((rows, cols // GROUPS), BF16),
-            pltpu.VMEM((rows, cols // GROUPS), BF16),
+            pltpu.VMEM((max(n_ask, 1), rows, cols // GROUPS), BF16),
+            pltpu.VMEM((max(n_ask, 1), rows, cols // GROUPS), BF16),
             pltpu.VMEM((rows, cols // GROUPS), BF16),
             pltpu.VMEM((rows, cols), F32),
             pltpu.VMEM(square, F32),
@@ -810,16 +835,16 @@
             pltpu.VMEM((n_fs, n_tp, 2, share, cols), BF16),
             pltpu.VMEM((others, share, out_cols), F32),
             pltpu.VMEM((others, CHUNKS, share, piece), BF16),
-            pltpu.VMEM((others, CHUNKS, share, piece), BF16),
             dma((1,)), dma((N_SMALL,)), dma((N_PROJ // 2 + 1,)),
             dma((others,)), dma((others * X_CHUNKS,)), dma((others * (n_tp - 1),)),
             dma((n_tp - 1,)), dma((1,)), dma((n_tp - 1,)), dma((n_tp - 1,)),
             dma((others,)), dma((others * n_sends,)),
             dma((n_sp,)), dma(((n_sp - 1) * n_kv,)),
             dma((1,)), dma((n_heads,)),
-            dma((n_tp - 1,)), dma((n_tp - 1,)), dma((2,)),
+            dma((n_tp - 1,)), dma((n_tp - 1,)), dma((max(2 * n_ask, 1),)),
             dma((n_fs * n_tp,)), dma((n_tp + others * n_tp * (2 + n_heads // GROUPS),)),
-            dma((others,)), dma((others * CHUNKS,)),
+            dma((others,)), dma((others,)),
+            pltpu.SemaphoreType.REGULAR,
         ],
         compiler_params=pltpu.CompilerParams(
             collective_id=0, has_side_effects=True, vmem_limit_bytes=60 * 1024 * 1024

time: 39.6 us -> 39 us (0.985)
  Pallas kernels: 38.8 us -> 38.1 us
    pallas_call x1, Pallas kernels: 38.8 us -> 38.1 us  [body(): pl.pallas_call(functools.partial(kernel, n_sp, n_fs, n_tp), out_shape=plt...]
where the time goes in v4:
time: 39 us; the launch traced here: 38.9 us
  Pallas kernels  38.1 us (98%)
  local copies, waits for them, and re-layouts  0.71 us (2%)
    pallas_call x1, Pallas kernels, body(): pl.pallas_call(functools.partial(kernel, n_sp, n_fs, n_tp), out_shape=plt...  38.1 us

profile of v4, /device:TPU:26, one launch (start us, length us, event | category | flops | bytes accessed | tf_op | source)
XLA Modules:
  0.0 38.9 jit_solution(3921250101183758662)
XLA Ops:
  0.0 38.1 %layer.1 = bf16[64,2048]{1,0:T(8,128)(2,1)S(1)} custom-call(bf16[128,1024]{1,0:T(8,128)(2,1)} %bitcast.6, f32[1,2048]{1,0:T(1,128)} %bitcast.7, bf16[1024,512]{1,0:T(8,128)(2,1)} %w_k.1, bf16[1024,512]{1,0:T(8,128)(2,1)} %w_v.1, bf16[1024,512]{1,0:T(8,128)(2,1)} %w_f.1, bf16[1024,512]{1,0:T(8,128)(2,1)} %w_i.1, bf16[1024,512]{1,0:T(8,128)(2,1)} %w_q.1, ...), custom_call_target="tpu_custom_call" | custom-call | tf_op jit(solution)/shard_map/layer/pallas_call | solution.py:798
  38.1 0.7 %copy.15 = bf16[1,64,2048]{2,1,0:T(8,128)(2,1)} copy(bf16[1,64,2048]{2,1,0:T(8,128)(2,1)S(1)} %bitcast.5) | data formatting | bytes 524288

commit v5 on v4

--- a/solution.py
+++ b/solution.py
@@ -17,9 +17,11 @@
 KEY, VALUE, FORGET, INPUT, QUERY, READ = range(N_PROJ)
 GROUPS = 2
 CHUNKS = 4
-X_CHUNKS = 4
+X_SPLIT = (1,2,2,3)
+X_CHUNKS = len(X_SPLIT)
 N_SMALL = 4
 N_ASK = 2
+SUM_ROWS = 16
 
 
 def dot_nn(a, b):
@@ -48,6 +50,14 @@
     units += [(QUERY, g * g_cols) for g in range(GROUPS - 1)]
     units += [(READ, g * g_cols) for g in range(GROUPS)]
     return units
+
+
+def ask_list(n_sp):
+    first = n_sp - min(N_ASK, n_sp - 2)
+    pairs = [(asker, 0) for asker in range(first, n_sp)]
+    if n_sp > 2:
+        pairs.append((n_sp - 1, n_sp - 2))
+    return pairs
 
 
 def kernel(
@@ -71,7 +81,7 @@
     g_cols = cols // GROUPS
     g_heads = n_heads // GROUPS
     n_kv = X_CHUNKS + 2 * (GROUPS - 1)
-    x_rows = rows // X_CHUNKS
+    x_edges = [rows * sum(X_SPLIT[:c]) // sum(X_SPLIT) for c in range(X_CHUNKS + 1)]
     relay = 0
     is_relay = tp == relay
     has_next = sp < n_sp - 1
@@ -79,6 +89,8 @@
     n_ask = min(N_ASK, n_sp - 2)
     first_ask = n_sp - n_ask
     asks = sp >= first_ask
+    asked = ask_list(n_sp)
+    near_owner = n_sp - 2 if n_sp > 2 else -1
     last = GROUPS - 1
     near = sp < 3
     far = sp >= 3
@@ -152,7 +164,7 @@
         return pl.ds(pl.multiple_of(lax.rem(f_index * feat_f, feat_t), LANES), feat_f)
 
     def x_part(c):
-        return pl.ds(c * x_rows, x_rows)
+        return pl.ds(x_edges[c], x_edges[c + 1] - x_edges[c])
 
     def x_copy(df, c):
         return pltpu.make_async_remote_copy(
@@ -251,11 +263,15 @@
     def own_product(w, cut):
         acc[w, :, cut] = dot_nn(xg[0], wbuf[w, :, cut])
 
+    @pl.when(sp == 0)
+    def _():
+        st_in[...] = jnp.zeros_like(st_in)
+
     w_wait(KEY)
     own_product(KEY, group(0))
     own_product(VALUE, group(0))
     for c in range(X_CHUNKS):
-        part = slice(c * x_rows, (c + 1) * x_rows)
+        part = slice(x_edges[c], x_edges[c + 1])
         for df in range(1, n_fs):
             slot = fs_at(df)
             land(xt.at[slot, x_part(c)], x_recv.at[(df - 1) * X_CHUNKS + c])
@@ -310,7 +326,7 @@
             kv_copy(sp, c).start()
 
     def finish_first(c):
-        part = slice(c * x_rows, (c + 1) * x_rows)
+        part = slice(x_edges[c], x_edges[c + 1])
         for df in range(1, n_fs):
             first_copy(df, c).wait_recv()
         for w in (KEY, VALUE):
@@ -322,7 +338,11 @@
 
     def finish_kv(w, g):
         kv[sp, 2 * g + w] = finish(w, g)
-        send_kv(X_CHUNKS + 2 * (g - 1) + w)
+        goes_on = jnp.logical_and(has_next, sp != near_owner) if g == last else has_next
+
+        @pl.when(goes_on)
+        def _():
+            kv_copy(sp, X_CHUNKS + 2 * (g - 1) + w).start()
 
     def hand_on(step, c):
         kv_copy(sp - step, c).wait_recv()
@@ -334,48 +354,57 @@
         def _():
             kv_copy(sp - step, c).start()
 
-    def from_step(step, g):
-        return step + 1 if g == last and step >= first_ask else step
+    def arrives(step, g):
+        here = sp >= step
+        if g == last:
+            unasked = jnp.logical_or(sp < first_ask, sp > step)
+            here = jnp.logical_and(here, unasked if step > 1 else sp != near_owner + 1)
+        return here
 
     def hand_on_if(step, c):
         if step < n_sp:
             g = last if c in group_kv(last) else 0
-            pl.when(sp >= from_step(step, g))(functools.partial(hand_on, step, c))
+            pl.when(arrives(step, g))(functools.partial(hand_on, step, c))
 
     @pl.when(has_next)
     def _():
         pl.semaphore_wait(ready, 1)
 
+    def send_if(condition, w, g):
+        pl.when(condition)(functools.partial(send_unit, w, g))
+
+    first = sp == 0
+    w_wait(QUERY)
+    partials(QUERY, 0, cols)
+    send_if(asks, QUERY, last)
+    finish_first(0)
+    for w in (KEY, VALUE):
+        partials(w, g_cols, cols - g_cols)
+        for g in range(1, GROUPS):
+            send_if(has_prev, w, g)
+    finish_first(1)
     w_wait(FORGET)
-    quarter = X_CHUNKS // 4
     for w in (FORGET, INPUT):
         partials(w, 0, cols)
         send_unit(w, 0)
-        for c in range(quarter):
-            finish_first((w - FORGET) * quarter + c)
-    w_wait(QUERY)
-    partials(QUERY, 0, cols)
-    pl.when(has_prev)(functools.partial(send_unit, QUERY, last))
-    for w in (KEY, VALUE):
-        partials(w, g_cols, cols - g_cols)
-        for g in range(1, GROUPS):
-            send_unit(w, g)
-        for c in range(quarter):
-            finish_first((2 + w) * quarter + c)
+        finish_first(w)
+    for c in range(INPUT + 1, X_CHUNKS):
+        finish_first(c)
     for w in (FORGET, INPUT):
         for g in range(1, GROUPS):
             send_unit(w, g)
-    pl.when(sp == 0)(functools.partial(send_unit, QUERY, last))
+    for w in (KEY, VALUE):
+        for g in range(1, GROUPS):
+            send_if(first, w, g)
+    send_if(jnp.logical_not(asks), QUERY, last)
     for g in range(last):
         send_unit(QUERY, g)
     partials(READ, 0, cols)
     for g in range(GROUPS):
         send_unit(READ, g)
-    for w in (FORGET, INPUT):
-        own_product(w, slice(0, cols))
     for w in (KEY, VALUE):
         own_product(w, slice(g_cols, cols))
-    for w in (QUERY, READ):
+    for w in (QUERY, FORGET, INPUT, READ):
         own_product(w, slice(0, cols))
 
     def o_copy(dt):
@@ -466,15 +495,15 @@
     early = pl.ds(0, last * g_cols)
 
     def h_sem(df, dt, mark):
-        return h_recv.at[dt if df == 0 else n_tp + ((df - 1) * n_tp + dt) * n_land + mark]
+        return h_recv.at[dt - 1 if df == 0 else n_tp - 1 + ((df - 1) * n_tp + dt) * n_land + mark]
 
     def h_copy(df, dt, kind, first, count, mark):
         lands = (n_tp - dt) % n_tp
         lanes = pl.ds(first, count)
         return pltpu.make_async_remote_copy(
             src_ref=heads.at[kind, pl.ds(pl.multiple_of(tp_at(dt) * share, share), share), lanes],
-            dst_ref=hrecv.at[df, lands, kind, :, lanes],
-            send_sem=h_send.at[df * n_tp + dt], recv_sem=h_sem(df, lands, mark),
+            dst_ref=hrecv.at[df * n_tp + lands, kind, :, lanes],
+            send_sem=h_send.at[0], recv_sem=h_sem(df, lands, mark),
             device_id={"fs": fs_at(df), "tp": tp_at(dt)}, device_id_type=MESH,
         )
 
@@ -491,11 +520,7 @@
     def finish_rec(h):
         lanes = lanes_of(h)
 
-        @pl.when(has_prev)
-        def _():
-            loc[:, lanes] += dot_nt(qdec[:, lanes], st_in[h])
-
-        raw = loc[:, lanes]
+        raw = loc[:, lanes] + dot_nt(qdec[:, lanes], st_in[h])
         norm = lax.rsqrt(jnp.mean(raw * raw, axis=1, keepdims=True) + norm_eps)
         heads[1, :, lanes] = (raw * norm * out_gain[...]).astype(BF16)
 
@@ -521,14 +546,15 @@
         log_stick = z + keep
         if diagonal:
             keep = jnp.where(strict, keep, 0.0)
-        both = dot_nn(jnp.concatenate(halves(keep), axis=1), sums)
+        keeps = jnp.concatenate(halves(keep), axis=1)
+        both = dot_nn(keeps, sums)
         stick = jnp.exp(log_stick + both[:, :rows])
         if diagonal:
             stick = jnp.where(strict, stick, 0.0)
-        return stick.astype(BF16), both
+        return stick.astype(BF16), both, keeps
 
     def attend(slot, g, diagonal):
-        stick, both = sticks(qbuf.at[:, group(g)], slot, g, diagonal)
+        stick, both, _ = sticks(qbuf.at[:, group(g)], slot, g, diagonal)
         for i, h in enumerate(heads_of(g)):
             mine = slice(i * rows, (i + 1) * rows)
             value = dot_nn(stick[mine], kv[slot, 2 * g + 1, :, lanes_of(i)])
@@ -542,7 +568,7 @@
 
     def attend_if(step, g):
         if step < n_sp:
-            pl.when(sp >= from_step(step, g))(functools.partial(attend, sp - step, g, False))
+            pl.when(arrives(step, g))(functools.partial(attend, sp - step, g, False))
 
     def attend_rest(g):
         def block(step, carry):
@@ -554,69 +580,112 @@
         end = jnp.where(asks, sp, sp + 1) if g == last else sp + 1
         lax.fori_loop(3, end, block, 0)
 
-    def q_copy(asker):
-        return pltpu.make_async_remote_copy(
-            src_ref=qbuf.at[:, pl.ds(last * g_cols, g_cols)], dst_ref=q_back.at[asker],
-            send_sem=b_sem.at[asker], recv_sem=b_sem.at[asker], device_id={"sp": 0}, device_id_type=MESH,
-        )
-
-    def v_copy(asker):
-        return pltpu.make_async_remote_copy(
-            src_ref=v_back.at[asker], dst_ref=v_far,
-            send_sem=b_sem.at[n_ask + asker], recv_sem=b_sem.at[n_ask + asker],
-            device_id={"sp": first_ask + asker}, device_id_type=MESH,
+    def place(pair):
+        asker, owner = asked[pair]
+        return asker - first_ask if owner == 0 else 0
+
+    def q_copy(pair):
+        return pltpu.make_async_remote_copy(
+            src_ref=qbuf.at[:, pl.ds(last * g_cols, g_cols)], dst_ref=q_back.at[place(pair)],
+            send_sem=b_sem.at[pair], recv_sem=b_sem.at[pair],
+            device_id={"sp": asked[pair][1]}, device_id_type=MESH,
+        )
+
+    def v_copy(pair):
+        asker, owner = asked[pair]
+        sem = b_sem.at[len(asked) + pair]
+        count = pl.ds(0, rows if owner == 0 else rows + SUM_ROWS)
+        return pltpu.make_async_remote_copy(
+            src_ref=v_back.at[place(pair), count], dst_ref=v_far.at[0 if owner == 0 else 1, count],
+            send_sem=sem, recv_sem=sem, device_id={"sp": asker}, device_id_type=MESH,
         )
 
     def ask_back():
-        for asker in range(n_ask):
-            @pl.when(sp == first_ask + asker)
-            def _(asker=asker):
-                q_copy(asker).start()
-
-    def answer():
-        for asker in reversed(range(n_ask)):
-            q_copy(asker).wait_recv()
-            stick, _ = sticks(q_back.at[asker], 0, last, False)
-            for i in range(g_heads):
-                value = dot_nn(stick[i * rows:(i + 1) * rows], kv[0, 2 * last + 1, :, lanes_of(i)])
-                v_back[asker, :, lanes_of(i)] = value.astype(BF16)
-            v_copy(asker).start()
-
-    def take_answer():
-        for asker in range(n_ask):
-            @pl.when(sp == first_ask + asker)
-            def _(asker=asker):
-                v_copy(asker).wait_recv()
-
+        for pair in reversed(range(len(asked))):
+            @pl.when(sp == asked[pair][0])
+            def _(pair=pair):
+                q_copy(pair).start()
+
+    def answer(pair):
+        owner, mine = asked[pair][1], place(pair)
+        q_copy(pair).wait_recv()
+        stick, _, keeps = sticks(q_back.at[mine], owner, last, False)
+        for i in range(g_heads):
+            part = slice(i * rows, (i + 1) * rows)
+            value = dot_nn(stick[part], kv[owner, 2 * last + 1, :, lanes_of(i)])
+            v_back[mine, 0:rows, lanes_of(i)] = value.astype(BF16)
+            if owner > 0:
+                sums_t = dot_nt(jnp.ones((SUM_ROWS // 2, keeps.shape[1]), BF16), keeps[part])
+                high = sums_t.astype(BF16).astype(F32)
+                pieces = jnp.concatenate([high, sums_t - high], axis=0)
+                v_back[mine, rows:rows + SUM_ROWS, lanes_of(i)] = pieces.astype(BF16)
+        v_copy(pair).start()
+
+    def answers(near_ones):
+        for pair in reversed(range(len(asked))):
+            owner = asked[pair][1]
+            if (owner > 0) == near_ones:
+                pl.when(sp == owner)(functools.partial(answer, pair))
+
+    def take(pair):
+        slot = 0 if asked[pair][1] == 0 else 1
+        v_copy(pair).wait_recv()
         for i, h in enumerate(heads_of(last)):
-            att[:, lanes_of(h)] += v_far[:, lanes_of(i)].astype(F32) * jnp.exp(run[h])
-
+            past = run[h]
+            value = v_far[slot, 0:rows, lanes_of(i)].astype(F32)
+            att[:, lanes_of(h)] += value * jnp.exp(past)
+            if slot > 0:
+                spread = jnp.full((SUM_ROWS, LANES), 2.0 / SUM_ROWS, BF16)
+                run[h] = past + dot_tn(v_far[slot, rows:rows + SUM_ROWS, lanes_of(i)], spread)
+
+    def take_answers(near_ones):
+        for pair, (asker, owner) in enumerate(asked):
+            if (owner > 0) == near_ones:
+                pl.when(sp == asker)(functools.partial(take, pair))
+
+    def last_queries():
+        qbuf[:, group(last)] = finish(QUERY, last)
+
+    def late_keys():
+        for g in range(1, GROUPS):
+            for w in (KEY, VALUE):
+                finish_kv(w, g)
+
+    def last_hop():
+        for g in range(1, GROUPS):
+            for c in group_kv(g):
+                hand_on(1, c)
+
+    pl.when(asks)(last_queries)
     for c in group_kv(0):
         hand_on_if(1, c)
-    gates(0)
-    local_state(0)
-
-    def last_queries():
-        qbuf[:, group(last)] = finish(QUERY, last)
-
-    pl.when(has_prev)(last_queries)
+    pl.when(has_prev)(late_keys)
     for c in group_kv(0):
         hand_on_if(2, c)
         if c == 0 and n_sp <= 4:
             ask_back()
-    for g in range(1, GROUPS):
-        for w in (KEY, VALUE):
-            finish_kv(w, g)
+    gates(0)
+    local_state(0)
     state_step_if(1, 0)
+    pl.when(jnp.logical_and(sp > 1, sp != near_owner + 1))(last_hop)
     for g in range(1, GROUPS):
         gates(g)
-        hand_on_if(1, group_kv(g)[0])
+        state_step_if(2, g - 1)
+        if n_sp <= 4:
+            answers(True)
         local_state(g)
-        hand_on_if(1, group_kv(g)[1])
-    state_step_if(2, 0)
-    pl.when(sp == 0)(last_queries)
-    for g in range(1, GROUPS):
         state_step_if(1, g)
+    pl.when(first)(late_keys)
+    pl.when(jnp.logical_not(asks))(last_queries)
+    state_step_if(2, last)
+    attend(sp, last, True)
+
+    @pl.when(first)
+    def _():
+        send_attn(last)
+
+    if n_sp <= 4:
+        answers(False)
     for g in range(last):
         qbuf[:, group(g)] = finish(QUERY, g)
         attend(sp, g, True)
@@ -626,48 +695,35 @@
         send_attn(g)
     if n_sp > 4:
         ask_back()
-    if n_ask:
-        pl.when(sp == 0)(answer)
-    for g in range(1, GROUPS):
-        attend(sp, g, True)
-        attend_if(1, g)
-
-        @pl.when(sp < 2)
-        def _(g=g):
-            send_attn(g)
-
-    state_step_if(2, last, 0)
+        answers(True)
+        answers(False)
+    pl.when(sp == 1)(last_hop)
+    attend_if(1, last)
+
+    @pl.when(sp == 1)
+    def _():
+        send_attn(last)
+
     read_local(0)
-
-    @pl.when(near)
-    def _():
-        send_rec(0)
-
-    for g in range(1, GROUPS):
-        read_local(g)
-        if g == last:
-            state_step_if(2, g, 1)
-        hand_on_if(2, group_kv(g)[0])
-        hand_on_if(2, group_kv(g)[1])
-        attend_if(2, g)
-
-        @pl.when(far)
-        def _(g=g):
-            attend_rest(g)
-
-        if g == last:
-            pl.when(asks)(take_answer)
-
-        @pl.when(sp >= 2)
-        def _(g=g):
-            send_attn(g)
-
-        @pl.when(far)
-        def _(g=g):
-            state_steps(g - 1)
-            send_rec(g - 1)
-
-        send_rec(g)
+    pl.when(far)(functools.partial(state_steps, 0))
+    send_rec(0)
+    read_local(last)
+    take_answers(True)
+    for c in group_kv(last):
+        hand_on_if(2, c)
+    attend_if(2, last)
+
+    @pl.when(far)
+    def _():
+        attend_rest(last)
+
+    take_answers(False)
+
+    @pl.when(sp >= 2)
+    def _():
+        send_attn(last)
+
+    send_rec(last)
 
     for dt in range(1, n_tp):
         other = tp_at(dt)
@@ -691,7 +747,7 @@
             if df == 0 and dt == 0:
                 left = heads[kind, pl.ds(pl.multiple_of(tp * share, share), share), lanes]
             else:
-                left = hrecv[df, dt, kind, :, lanes]
+                left = hrecv[df * n_tp + dt, kind, :, lanes]
             term = dot_nn(left, obuf[tp_at(dt), kind, lanes, cut])
             value = term if value is None else value + term
         return value
@@ -700,7 +756,7 @@
     final = lanes_of(n_heads - 1)
     for df in range(1, n_fs):
         for dt in range(n_tp):
-            land(hrecv.at[df, dt, :, :, early], h_sem(df, dt, 0))
+            land(hrecv.at[df * n_tp + dt, :, :, early], h_sem(df, dt, 0))
         for kind in range(2):
             for g in range(last):
                 if kind == 0 and g == 0:
@@ -710,7 +766,7 @@
         marks = [(0, group(last))] + [(1, lanes_of(h)) for h in heads_of(last)]
         for mark, (kind, lanes) in enumerate(marks):
             for dt in range(n_tp):
-                land(hrecv.at[df, dt, kind, :, lanes], h_sem(df, dt, 1 + mark))
+                land(hrecv.at[df * n_tp + dt, kind, :, lanes], h_sem(df, dt, 1 + mark))
             if mark < len(marks) - 1:
                 part_acc[df - 1] += product(df, kind, lanes, whole)
         for k in range(CHUNKS):
@@ -718,7 +774,7 @@
             mix[df - 1, k] = (part_acc[df - 1, :, cut] + product(df, 1, final, cut)).astype(BF16)
             m_copy(df, k).start()
     for dt in range(1, n_tp):
-        land(hrecv.at[0, dt], h_sem(0, dt, 0))
+        land(hrecv.at[dt], h_sem(0, dt, 0))
     for k in range(CHUNKS):
         cut = slice(k * half, (k + 1) * half)
         value = product(0, 0, slice(0, cols), cut) + product(0, 1, slice(0, cols), cut)
@@ -742,33 +798,37 @@
 
         ss_copy(dt).wait_send()
         o_copy(dt).wait_send()
-    for df, dt in h_order:
-        land(hrecv.at[df, dt], h_send.at[df * n_tp + dt], True)
+    land(hrecv.at[pl.ds(1, n_fs * n_tp - 1)], h_send.at[0], True)
 
     @pl.when(has_next)
     def _():
         land(st_out, st_send.at[0], True)
 
         def drain(slot, carry):
-            land(kv.at[slot], kv_send.at[slot], True)
+            handed = jnp.logical_and(slot == 0, sp + 1 >= first_ask)
+            own = jnp.logical_and(slot == sp, sp == near_owner)
+            short = jnp.logical_or(handed, own)
+
+            @pl.when(short)
+            def _():
+                land(kv.at[slot, pl.ds(0, 2 * last)], kv_send.at[slot], True)
+
+            @pl.when(jnp.logical_not(short))
+            def _():
+                land(kv.at[slot], kv_send.at[slot], True)
+
             return carry
 
-        shorter = sp + 1 >= first_ask
-
-        @pl.when(shorter)
-        def _():
-            land(kv.at[0, pl.ds(0, 2 * last)], kv_send.at[0], True)
-
-        lax.fori_loop(jnp.where(shorter, 1, 0), sp + 1, drain, 0)
-
-    for asker in range(n_ask):
-        @pl.when(sp == first_ask + asker)
-        def _(asker=asker):
-            q_copy(asker).wait_send()
-
-        @pl.when(sp == 0)
-        def _(asker=asker):
-            v_copy(asker).wait_send()
+        lax.fori_loop(0, sp + 1, drain, 0)
+
+    for pair, (asker, owner) in enumerate(asked):
+        @pl.when(sp == asker)
+        def _(pair=pair):
+            q_copy(pair).wait_send()
+
+        @pl.when(sp == owner)
+        def _(pair=pair):
+            v_copy(pair).wait_send()
 
     for df in range(1, n_fs):
         land(mix.at[df - 1], m_recv.at[df - 1])
@@ -824,15 +884,15 @@
             pltpu.VMEM((rows, cols), F32),
             pltpu.VMEM((n_heads, rows, LANES), F32),
             pltpu.VMEM((max(n_ask, 1), rows, cols // GROUPS), BF16),
-            pltpu.VMEM((max(n_ask, 1), rows, cols // GROUPS), BF16),
-            pltpu.VMEM((rows, cols // GROUPS), BF16),
+            pltpu.VMEM((max(n_ask, 1), rows + SUM_ROWS, cols // GROUPS), BF16),
+            pltpu.VMEM((2, rows + SUM_ROWS, cols // GROUPS), BF16),
             pltpu.VMEM((rows, cols), F32),
             pltpu.VMEM(square, F32),
             pltpu.VMEM((n_heads, 8, LANES), F32),
             pltpu.VMEM(square, BF16),
             pltpu.VMEM(square, BF16),
             pltpu.VMEM((2, rows, cols), BF16),
-            pltpu.VMEM((n_fs, n_tp, 2, share, cols), BF16),
+            pltpu.VMEM((n_fs * n_tp, 2, share, cols), BF16),
             pltpu.VMEM((others, share, out_cols), F32),
             pltpu.VMEM((others, CHUNKS, share, piece), BF16),
             dma((1,)), dma((N_SMALL,)), dma((N_PROJ // 2 + 1,)),
@@ -841,8 +901,8 @@
             dma((others,)), dma((others * n_sends,)),
             dma((n_sp,)), dma(((n_sp - 1) * n_kv,)),
             dma((1,)), dma((n_heads,)),
-            dma((n_tp - 1,)), dma((n_tp - 1,)), dma((max(2 * n_ask, 1),)),
-            dma((n_fs * n_tp,)), dma((n_tp + others * n_tp * (2 + n_heads // GROUPS),)),
+            dma((n_tp - 1,)), dma((n_tp - 1,)), dma((max(2 * len(ask_list(n_sp)), 1),)),
+            dma((1,)), dma((n_tp - 1 + others * n_tp * (2 + n_heads // GROUPS),)),
             dma((others,)), dma((others,)),
             pltpu.SemaphoreType.REGULAR,
         ],

time: 39 us -> 38.2 us (0.979)
  Pallas kernels: 38.1 us -> 37.3 us
    pallas_call x1, Pallas kernels: 38.1 us -> 37.3 us  [body(): pl.pallas_call(functools.partial(kernel, n_sp, n_fs, n_tp), out_shape=plt...]
where the time goes in v5:
time: 38.2 us; the launch traced here: 38.1 us
  Pallas kernels  37.3 us (98%)
  local copies, waits for them, and re-layouts  0.71 us (2%)
    pallas_call x1, Pallas kernels, body(): pl.pallas_call(functools.partial(kernel, n_sp, n_fs, n_tp), out_shape=plt...  37.3 us

profile of v5, /device:TPU:26, one launch (start us, length us, event | category | flops | bytes accessed | tf_op | source)
XLA Modules:
  0.0 38.1 jit_solution(11248469502981569018)
XLA Ops:
  0.0 37.3 %layer.1 = bf16[64,2048]{1,0:T(8,128)(2,1)S(1)} custom-call(bf16[128,1024]{1,0:T(8,128)(2,1)} %bitcast.6, f32[1,2048]{1,0:T(1,128)} %bitcast.7, bf16[1024,512]{1,0:T(8,128)(2,1)} %w_k.1, bf16[1024,512]{1,0:T(8,128)(2,1)} %w_v.1, bf16[1024,512]{1,0:T(8,128)(2,1)} %w_f.1, bf16[1024,512]{1,0:T(8,128)(2,1)} %w_i.1, bf16[1024,512]{1,0:T(8,128)(2,1)} %w_q.1, ...), custom_call_target="tpu_custom_call" | custom-call | tf_op jit(solution)/shard_map/layer/pallas_call | solution.py:858
  37.3 0.7 %copy.15 = bf16[1,64,2048]{2,1,0:T(8,128)(2,1)} copy(bf16[1,64,2048]{2,1,0:T(8,128)(2,1)S(1)} %bitcast.5) | data formatting | bytes 524288

commit v6 on v5

--- a/solution.py
+++ b/solution.py
@@ -621,10 +621,10 @@
                 v_back[mine, rows:rows + SUM_ROWS, lanes_of(i)] = pieces.astype(BF16)
         v_copy(pair).start()
 
-    def answers(near_ones):
+    def answers(near_ones, ends=(False, True)):
         for pair in reversed(range(len(asked))):
-            owner = asked[pair][1]
-            if (owner > 0) == near_ones:
+            asker, owner = asked[pair]
+            if (owner > 0) == near_ones and (asker == n_sp - 1) in ends:
                 pl.when(sp == owner)(functools.partial(answer, pair))
 
     def take(pair):
@@ -677,7 +677,6 @@
         state_step_if(1, g)
     pl.when(first)(late_keys)
     pl.when(jnp.logical_not(asks))(last_queries)
-    state_step_if(2, last)
     attend(sp, last, True)
 
     @pl.when(first)
@@ -685,7 +684,7 @@
         send_attn(last)
 
     if n_sp <= 4:
-        answers(False)
+        answers(False, (False,))
     for g in range(last):
         qbuf[:, group(g)] = finish(QUERY, g)
         attend(sp, g, True)
@@ -697,6 +696,9 @@
         ask_back()
         answers(True)
         answers(False)
+    else:
+        answers(False, (True,))
+    state_step_if(2, last)
     pl.when(sp == 1)(last_hop)
     attend_if(1, last)
 
@@ -708,6 +710,7 @@
     pl.when(far)(functools.partial(state_steps, 0))
     send_rec(0)
     read_local(last)
+    pl.when(near)(functools.partial(send_rec, last))
     take_answers(True)
     for c in group_kv(last):
         hand_on_if(2, c)
@@ -723,7 +726,7 @@
     def _():
         send_attn(last)
 
-    send_rec(last)
+    pl.when(far)(functools.partial(send_rec, last))
 
     for dt in range(1, n_tp):
         other = tp_at(dt)

time: 38.2 us -> 38.2 us (level)
  no operation moved by 1% of the time
where the time goes in v6:
time: 38.2 us; the launch traced here: 38.1 us
  Pallas kernels  37.3 us (98%)
  local copies, waits for them, and re-layouts  0.71 us (2%)
    pallas_call x1, Pallas kernels, body(): pl.pallas_call(functools.partial(kernel, n_sp, n_fs, n_tp), out_shape=plt...  37.3 us

profile of v6, /device:TPU:26, one launch (start us, length us, event | category | flops | bytes accessed | tf_op | source)
XLA Modules:
  0.0 38.1 jit_solution(17926475972476546161)
XLA Ops:
  0.0 37.3 %layer.1 = bf16[64,2048]{1,0:T(8,128)(2,1)S(1)} custom-call(bf16[128,1024]{1,0:T(8,128)(2,1)} %bitcast.6, f32[1,2048]{1,0:T(1,128)} %bitcast.7, bf16[1024,512]{1,0:T(8,128)(2,1)} %w_k.1, bf16[1024,512]{1,0:T(8,128)(2,1)} %w_v.1, bf16[1024,512]{1,0:T(8,128)(2,1)} %w_f.1, bf16[1024,512]{1,0:T(8,128)(2,1)} %w_i.1, bf16[1024,512]{1,0:T(8,128)(2,1)} %w_q.1, ...), custom_call_target="tpu_custom_call" | custom-call | tf_op jit(solution)/shard_map/layer/pallas_call | solution.py:861
  37.3 0.7 %copy.15 = bf16[1,64,2048]{2,1,0:T(8,128)(2,1)} copy(bf16[1,64,2048]{2,1,0:T(8,128)(2,1)S(1)} %bitcast.5) | data formatting | bytes 524288
